TPU v7x, 32 devices: a whole 2x2x4 slice. The times are simulated.
32 devices in a mesh: grp: 2 (over y), ep: 4 (over z), tp: 4 (over x, core).
Axes of the slice: x: 2, y: 2, z: 4, core: 2. Of those that a mesh axis runs over, the one named last changes fastest.
Arguments:
- query_rows: bfloat16 [1536, 2048], P(('grp', 'ep'), 'tp'), parts along dimension 0, may hold values from -100 to 100
- projected_keys: bfloat16 [1536, 512], P(('grp', 'ep'), 'tp'), parts along dimension 0, may hold values from -100 to 100
- projected_values: bfloat16 [1536, 512], P(('grp', 'ep'), 'tp'), parts along dimension 0, may hold values from -6 to 6
- query_gain: float32 [128], replicated, may hold values from 0.3 to 6.5
- key_norm_gain: float32 [128], replicated, may hold values from 0.3 to 6.5
- out_proj: bfloat16 [2048, 2048], P('tp'), may hold values from -4 to 4
- mix_tokens: bfloat16 [4096, 2048], P(('grp', 'ep', 'tp')), parts along dimension 0, may hold values from -150 to 150
- norm_gain: float32 [2048], replicated, may hold values from 0.1 to 1.9
- expert_ids: int32 [4096, 2], P(('grp', 'ep', 'tp')), parts along dimension 0, may hold values from 0 to 3, all different within a row; in each aligned block of 128 rows (0 to 127, 128 to 255, ...) at most 96 rows name the same one
- expert_score: float32 [4096, 2], P(('grp', 'ep', 'tp')), parts along dimension 0, may hold values from -6 to 6
- gate_proj: bfloat16 [4, 2048, 2048], P('ep', None, 'tp'), may hold values from -0.125 to 0.125
- up_proj: bfloat16 [4, 2048, 2048], P('ep', None, 'tp'), may hold values from -0.125 to 0.125
- down_proj: bfloat16 [4, 2048, 2048], P('ep', 'tp'), may hold values from -0.125 to 0.125
Outputs:
- mixed_rows: bfloat16 [1536, 2048], P(('grp', 'ep', 'tp')), parts along dimension 0
- expert_out: bfloat16 [4096, 2048], P(('grp', 'ep', 'tp')), parts along dimension 0
There are 2 independent parts, one for each index of `grp`. A program takes and returns all parts, laid end to end along the dimension named above; an argument that names none is the same for every part. Nothing has to cross between parts.
Inputs may be any that keep to these rules, and one draw needn't show every extreme that they name: `expert_ids`: each row names 2 different experts. Within the rows of one device (aligned blocks of 128 rows) no expert is named more than 96 times, and in every draw some device names some expert exactly 96 times.
All inputs are finite; a program needn't handle non-finite values.
Results may differ from a plain program's by a relative error of at most 0.014.
The roundings to bfloat16 on the way count: a program that leaves them out, or rounds other values in their place, can miss the bound.
Values may be sent and summed in bfloat16 or wider, within the bound.
A program may use at most 128 MiB of HBM per device.

v0:
```python
import functools
import math

import jax
import jax.numpy as jnp
from jax import lax
from jax.experimental import pallas as pl
from jax.experimental.pallas import tpu as pltpu
from jax.sharding import PartitionSpec as P

GRID_W = 64


MESH = pl.DeviceIdType.MESH
EPS = 1e-06
THETA = 10000.0


def head_norm(vectors, gain):
    return vectors * lax.rsqrt(jnp.mean(vectors * vectors, axis=-1, keepdims=True) + EPS) * gain


def rotate_grid(vectors, token_positions):
    length, heads, head_dim = vectors.shape
    quarter = head_dim // 4
    freqs = 1.0 / THETA ** (jnp.arange(quarter, dtype=jnp.float32) * 4.0 / head_dim)
    grid_row = (token_positions // GRID_W).astype(jnp.float32)
    grid_col = (token_positions % GRID_W).astype(jnp.float32)
    angles = jnp.stack([grid_row[:, None] * freqs, grid_col[:, None] * freqs], axis=1)
    cosine = jnp.cos(angles)[:, None]
    sine = jnp.sin(angles)[:, None]
    halves = vectors.reshape(length, heads, 2, 2, quarter)
    first = halves[..., 0, :]
    second = halves[..., 1, :]
    turned = jnp.stack([first * cosine - second * sine, second * cosine + first * sine], axis=-2)
    return turned.reshape(length, heads, head_dim)


def prepare_inputs(raw_rows, gain, heads, token_positions):
    length = raw_rows.shape[0]
    head_dim = gain.shape[0]
    vectors = raw_rows.astype(jnp.float32).reshape(length, heads, head_dim)
    return rotate_grid(head_norm(vectors, gain), token_positions).astype(jnp.bfloat16)


def mixer_prepare(query_rows, projected_keys, projected_values, query_gain, key_norm_gain):
    length = query_rows.shape[0]
    head_dim = query_gain.shape[0]
    kv_heads = projected_keys.shape[1] // head_dim
    q_heads = query_rows.shape[1] // head_dim
    token_positions = lax.axis_index("ep") * length + jnp.arange(length, dtype=jnp.int32)
    query_matrix = prepare_inputs(query_rows, query_gain, q_heads, token_positions).reshape(
        length, q_heads * head_dim
    )
    keys_turned = prepare_inputs(projected_keys, key_norm_gain, kv_heads, token_positions).reshape(
        length, kv_heads * head_dim
    )
    return query_matrix, jnp.concatenate([keys_turned, projected_values], axis=1)


def attend_plain(query_matrix, own_pair, head_dim):
    length = query_matrix.shape[0]
    kv_heads = own_pair.shape[1] // (2 * head_dim)
    q_heads = query_matrix.shape[1] // head_dim
    queries_per_group = q_heads // kv_heads
    query_matrix = query_matrix.reshape(length, kv_heads, queries_per_group, head_dim)
    score_scale = head_dim ** (-0.5)
    initial = (
        jnp.full((kv_heads, queries_per_group, length), -1e30, jnp.float32),
        jnp.zeros((kv_heads, queries_per_group, length), jnp.float32),
        jnp.zeros((length, kv_heads, queries_per_group, head_dim), jnp.float32),
    )
    width = kv_heads * head_dim
    pair = lax.all_gather(own_pair, "ep", axis=0, tiled=True)
    key_piece = pair[:, :width]
    value_piece = pair[:, width:]
    piece_rows = key_piece.shape[0]
    step_rows = math.gcd(piece_rows, 1024)

    def one_block(block_index, running):
        run_max, run_sum, run_acc = running
        offset = block_index * step_rows
        key_block = lax.dynamic_slice_in_dim(key_piece, offset, step_rows, 0).reshape(
            step_rows, kv_heads, head_dim
        )
        value_block = lax.dynamic_slice_in_dim(value_piece, offset, step_rows, 0).reshape(
            step_rows, kv_heads, head_dim
        )
        scores = (
            jnp.einsum(
                "tkgd,skd->kgts", query_matrix, key_block, preferred_element_type=jnp.float32
            )
            * score_scale
        )
        new_max = jnp.maximum(run_max, jnp.max(scores, axis=-1))
        factor = jnp.exp(run_max - new_max)
        weights = jnp.exp(scores - new_max[..., None])
        run_sum = run_sum * factor + jnp.sum(weights, axis=-1)
        update = jnp.einsum(
            "kgts,skd->tkgd",
            weights.astype(jnp.bfloat16),
            value_block,
            preferred_element_type=jnp.float32,
        )
        run_acc = run_acc * jnp.transpose(factor, (2, 0, 1))[..., None] + update
        return (new_max, run_sum, run_acc)

    run_max, run_sum, run_acc = lax.fori_loop(0, piece_rows // step_rows, one_block, initial)
    return (
        (run_acc / jnp.transpose(run_sum, (2, 0, 1))[..., None])
        .astype(jnp.bfloat16)
        .reshape(length, q_heads * head_dim)
    )


def flip(index, bits):
    result, place = 0, 1
    for _ in range(8):
        mine = (index // place) % 2
        result = result + place * ((1 - mine) if bits & place else mine)
        place *= 2
    return result


def exchange_kernel(
    steps,
    out_ref,
    gate_ref,
    up_ref,
    down_ref,
    query_ref,
    pair_ref,
    back_ref,
    heads_ref,
    rows,
    act,
    part,
    from_core,
    to_x,
    from_x,
    total,
    pairs,
    zs,
    zr,
    xs,
    xr,
    cs,
    cr,
    ps,
    pr,
    qs,
    qr,
    bs,
    br,
    ks,
    kr,
):
    me = lax.axis_index("ep")
    lane = lax.axis_index("tp")
    peers = [flip(me, k) for k in range(steps)]
    core, across = flip(lane, 1), flip(lane, 2)
    cap, width = out_ref.shape[1], out_ref.shape[2]
    hidden = gate_ref.shape[1]
    tile = math.gcd(hidden, 256)
    tile_out = math.gcd(width, 256)

    barrier = pltpu.get_barrier_semaphore()
    friends = [{"ep": peers[k], "tp": lane} for k in range(1, steps)]
    friends += [{"ep": me, "tp": core}, {"ep": me, "tp": across}]
    for friend in friends:
        pl.semaphore_signal(barrier, inc=1, device_id=friend, device_id_type=MESH)
    pl.semaphore_wait(barrier, len(friends))

    def remote(src, dst, send, recv, ep_to, tp_to):
        return pltpu.make_async_remote_copy(
            src_ref=src,
            dst_ref=dst,
            send_sem=send,
            recv_sem=recv,
            device_id={"ep": ep_to, "tp": tp_to},
            device_id_type=MESH,
        )

    z_in = [None] + [
        remote(out_ref.at[peers[k]], rows.at[k, 0], zs.at[k], zr.at[k], peers[k], lane)
        for k in range(1, steps)
    ]
    kv_in = [None] + [
        remote(pair_ref, pairs.at[k], ks.at[k], kr.at[k], peers[k], lane)
        for k in range(1, steps)
    ]
    x_in = [
        remote(
            out_ref.at[me] if k == 0 else rows.at[k, 0],
            rows.at[k, 1],
            xs.at[k],
            xr.at[k],
            me,
            across,
        )
        for k in range(steps)
    ]
    c_in = [
        remote(
            rows.at[k, pl.ds(0, 2)], rows.at[k, pl.ds(2, 2)], cs.at[k], cr.at[k], me, core
        )
        for k in range(steps)
    ]
    c_out = [
        remote(part.at[k, pl.ds(2, 2)], from_core.at[k], ps.at[k], pr.at[k], me, core)
        for k in range(steps)
    ]
    x_out = [
        remote(to_x.at[k], from_x.at[k], qs.at[k], qr.at[k], me, across) for k in range(steps)
    ]
    z_out = [None] + [
        remote(total.at[k], back_ref.at[me], bs.at[k], br.at[k], peers[k], lane)
        for k in range(1, steps)
    ]

    def stage_a(k):
        if k > 0:
            z_in[k].wait_recv()
        x_in[k].start()

    def stage_b(k):
        x_in[k].wait_recv()
        c_in[k].start()

    def stage_c(k):
        c_in[k].wait_recv()

        @pl.loop(0, hidden // tile)
        def _(i):
            cols = pl.ds(pl.multiple_of(i * tile, tile), tile)
            block = rows[k].reshape(4 * cap, width)
            gate = jnp.dot(block, gate_ref[:, cols], preferred_element_type=jnp.float32)
            up = jnp.dot(block, up_ref[:, cols], preferred_element_type=jnp.float32)
            act[:, cols] = (gate / (1.0 + jnp.exp(-gate)) * up).astype(jnp.bfloat16)

        @pl.loop(0, width // tile_out)
        def _(i):
            cols = pl.ds(pl.multiple_of(i * tile_out, tile_out), tile_out)
            summed = jnp.dot(act[...], down_ref[:, cols], preferred_element_type=jnp.float32)
            part[k, :, :, cols] = summed.astype(jnp.bfloat16).reshape(4, cap, tile_out)

        c_out[k].start()

    def stage_d(k):
        c_out[k].wait_recv()
        to_x[k] = (
            part[k, 1].astype(jnp.float32) + from_core[k, 1].astype(jnp.float32)
        ).astype(jnp.bfloat16)
        x_out[k].start()

    def stage_e(k):
        x_out[k].wait_recv()
        summed = (
            part[k, 0].astype(jnp.float32)
            + from_core[k, 0].astype(jnp.float32)
            + from_x[k].astype(jnp.float32)
        ).astype(jnp.bfloat16)
        if k == 0:
            back_ref[me] = summed
        else:
            total[k] = summed
            z_out[k].start()

    def attend():
        for k in range(1, steps):
            kv_in[k].wait_recv()
        held = steps * pair_ref.shape[0]
        dim = pair_ref.shape[1] // 2
        keys = pairs[:, :, :dim].reshape(held, dim)
        values = pairs[:, :, dim:].reshape(held, dim)
        for head in range(query_ref.shape[1] // dim):
            cols = slice(head * dim, (head + 1) * dim)
            scores = (
                lax.dot_general(
                    query_ref[:, cols],
                    keys,
                    (((1,), (1,)), ((), ())),
                    preferred_element_type=jnp.float32,
                )
                * dim ** (-0.5)
            )
            probs = jnp.exp(scores - jnp.max(scores, axis=-1, keepdims=True))
            amount = jnp.sum(probs, axis=-1, keepdims=True)
            summed = jnp.dot(
                probs.astype(jnp.bfloat16), values, preferred_element_type=jnp.float32
            )
            heads_ref[:, cols] = (summed / amount).astype(jnp.bfloat16)

    for k in range(1, steps):
        kv_in[k].start()
        z_in[k].start()
    rows[0, 0] = out_ref[me]
    pairs[0] = pair_ref[...]
    stage_a(0)
    stage_b(0)
    for k in range(steps):
        if k > 0:
            stage_d(k - 1)
        if k == 1:
            attend()
        if k + 1 < steps:
            stage_a(k + 1)
        stage_c(k)
        if k > 0:
            stage_e(k - 1)
        if k + 1 < steps:
            stage_b(k + 1)
    stage_d(steps - 1)
    stage_e(steps - 1)
    for k in range(steps):
        if k > 0:
            z_out[k].wait_recv()
            z_in[k].wait_send()
            kv_in[k].wait_send()
            z_out[k].wait_send()
        for copy in (x_in[k], c_in[k], c_out[k], x_out[k]):
            copy.wait_send()


def exchange(outgoing, gate, up, down, queries, pair):
    steps, cap, width = outgoing.shape
    hidden = gate.shape[1]
    vmem = pl.BlockSpec(memory_space=pltpu.VMEM)
    kind = jnp.bfloat16
    return pl.pallas_call(
        functools.partial(exchange_kernel, steps),
        out_shape=(
            jax.ShapeDtypeStruct((steps, cap, width), kind),
            jax.ShapeDtypeStruct(queries.shape, kind),
        ),
        in_specs=[vmem] * 6,
        out_specs=(vmem, vmem),
        scratch_shapes=[
            pltpu.VMEM((steps, 4, cap, width), kind),
            pltpu.VMEM((4 * cap, hidden), kind),
            pltpu.VMEM((steps, 4, cap, width), kind),
            pltpu.VMEM((steps, 2, cap, width), kind),
            pltpu.VMEM((steps, cap, width), kind),
            pltpu.VMEM((steps, cap, width), kind),
            pltpu.VMEM((steps, cap, width), kind),
            pltpu.VMEM((steps,) + pair.shape, kind),
        ]
        + [pltpu.SemaphoreType.DMA((steps,))] * 14,
        compiler_params=pltpu.CompilerParams(
            collective_id=0, has_side_effects=True, vmem_limit_bytes=60 * 1024 * 1024
        ),
    )(outgoing, gate, up, down, queries, pair)


def fits_exchange(lanes, steps, local_experts, cap, width, hidden, length, kv_heads):
    blocks = 14 * steps * cap * width * 2 + 3 * width * hidden * 2
    return (
        lanes == 4
        and local_experts == 1
        and steps & (steps - 1) == 0
        and 1 < steps <= 8
        and kv_heads == 1
        and length % 16 == 0
        and length <= 256
        and cap % 16 == 0
        and blocks < 44 * 1024 * 1024
    )


def exchange_plain(outgoing, gate_proj, up_proj, down_proj):
    rows_in = lax.all_gather(
        lax.all_to_all(outgoing, "ep", split_axis=0, concat_axis=0, tiled=True),
        "tp",
        axis=0,
        tiled=True,
    )
    gate_out = jnp.einsum("secd,edf->secf", rows_in, gate_proj, preferred_element_type=jnp.float32)
    up_out = jnp.einsum("secd,edf->secf", rows_in, up_proj, preferred_element_type=jnp.float32)
    active = (jax.nn.silu(gate_out) * up_out).astype(jnp.bfloat16)
    summed = lax.psum_scatter(
        jnp.einsum("secf,efd->secd", active, down_proj, preferred_element_type=jnp.float32).astype(
            jnp.bfloat16
        ),
        "tp",
        scatter_dimension=0,
        tiled=True,
    )
    return lax.all_to_all(summed, "ep", split_axis=0, concat_axis=0, tiled=True)


def both_halves(
    query_rows,
    projected_keys,
    projected_values,
    query_gain,
    key_norm_gain,
    out_proj,
    mix_tokens,
    norm_gain,
    expert_ids,
    expert_score,
    gate_proj,
    up_proj,
    down_proj,
):
    length, model_dim = mix_tokens.shape
    top_count = expert_ids.shape[1]
    local_experts = gate_proj.shape[0]
    expert_axis = lax.axis_size("ep")
    experts_all = expert_axis * local_experts
    capacity = length * top_count * 3 // (2 * experts_all)
    values_b = mix_tokens.astype(jnp.float32)
    normed = (
        values_b
        * lax.rsqrt(jnp.mean(values_b * values_b, axis=-1, keepdims=True) + EPS)
        * norm_gain
    ).astype(jnp.bfloat16)
    flat = expert_ids.reshape(length * top_count)
    onehot = (flat[:, None] == jnp.arange(experts_all, dtype=jnp.int32)).astype(jnp.int32)
    slots = jnp.sum((jnp.cumsum(onehot, axis=0) - onehot) * onehot, axis=1)
    target = flat * capacity + slots
    placed = (target[:, None] == jnp.arange(experts_all * capacity, dtype=jnp.int32)).astype(
        jnp.int32
    )
    placed = jnp.sum(placed.reshape(length, top_count, experts_all * capacity), axis=1).astype(
        jnp.bfloat16
    )
    outgoing = jnp.einsum("re,rd->ed", placed, normed, preferred_element_type=jnp.float32).astype(
        jnp.bfloat16
    )
    outgoing = outgoing.reshape(expert_axis, local_experts, capacity, model_dim)
    lanes = lax.axis_size("tp")
    head_dim = query_gain.shape[0]
    queries, pair = mixer_prepare(
        query_rows, projected_keys, projected_values, query_gain, key_norm_gain
    )
    if fits_exchange(
        lanes,
        expert_axis,
        local_experts,
        capacity,
        model_dim,
        gate_proj.shape[2],
        queries.shape[0],
        pair.shape[1] // (2 * head_dim),
    ):
        returned, heads_out = exchange(
            outgoing.reshape(expert_axis, capacity, model_dim),
            gate_proj.reshape(gate_proj.shape[1:]),
            up_proj.reshape(up_proj.shape[1:]),
            down_proj.reshape(down_proj.shape[1:]),
            queries,
            pair,
        )
    else:
        heads_out = attend_plain(queries, pair, head_dim)
        returned = exchange_plain(outgoing, gate_proj, up_proj, down_proj)
    head_partial = jnp.dot(heads_out, out_proj, preferred_element_type=jnp.float32).astype(
        jnp.bfloat16
    )
    pieces = lax.all_to_all(
        head_partial.reshape(lanes, -1, head_partial.shape[1]),
        "tp",
        split_axis=0,
        concat_axis=0,
        tiled=True,
    )
    mixed_rows = jnp.sum(pieces.astype(jnp.float32), axis=0).astype(jnp.bfloat16)
    results = returned.reshape(experts_all * capacity, model_dim)
    first_weight = jax.nn.sigmoid(expert_score[:, 0] - expert_score[:, 1])
    picks = target.reshape(length, top_count)
    chosen = [
        jnp.dot(
            (picks[:, k : k + 1] == jnp.arange(experts_all * capacity, dtype=jnp.int32)).astype(
                jnp.bfloat16
            ),
            results,
            preferred_element_type=jnp.float32,
        )
        for k in range(2)
    ]
    combined = first_weight[:, None] * chosen[0] + (1.0 - first_weight)[:, None] * chosen[1]
    return (mixed_rows, combined.astype(jnp.bfloat16))


def local(
    query_rows,
    projected_keys,
    projected_values,
    query_gain,
    key_norm_gain,
    out_proj,
    mix_tokens,
    norm_gain,
    expert_ids,
    expert_score,
    gate_proj,
    up_proj,
    down_proj,
):
    return both_halves(
        query_rows,
        projected_keys,
        projected_values,
        query_gain,
        key_norm_gain,
        out_proj,
        mix_tokens,
        norm_gain,
        expert_ids,
        expert_score,
        gate_proj,
        up_proj,
        down_proj,
    )


def solution(mesh):
    in_specs = (
        P(("grp", "ep"), "tp"),
        P(("grp", "ep"), "tp"),
        P(("grp", "ep"), "tp"),
        P(),
        P(),
        P("tp", None),
        P(("grp", "ep", "tp"), None),
        P(),
        P(("grp", "ep", "tp"), None),
        P(("grp", "ep", "tp"), None),
        P("ep", None, "tp"),
        P("ep", None, "tp"),
        P("ep", "tp", None),
    )
    out_specs = (P(("grp", "ep", "tp"), None), P(("grp", "ep", "tp"), None))
    return jax.shard_map(local, mesh=mesh, in_specs=in_specs, out_specs=out_specs, check_vma=False)
```

profile of v0, /device:TPU:8, one launch (start us, length us, event | category | flops | bytes accessed | tf_op | source)
XLA Modules:
  0.0 143.4 jit_solution(9708661730634202304)
XLA Ops:
  0.6 0.0 copy-start
  0.7 0.9 copy.52
  1.6 0.1 eq.76
  1.7 0.1 eq.72
  1.9 1.1 copy.57
  3.0 0.1 bitcast_reduce_fusion
  3.0 0.0 copy-start.3
  3.1 0.7 mul.253
  3.8 0.1 fusion.17
  3.9 0.0 copy-start.8
  3.9 0.2 fusion.16
  4.2 0.1 multiply_multiply_fusion
  4.3 0.0 copy-start.6
  4.3 0.0 copy-start.2
  4.3 0.1 subtract_convert_fusion
  4.4 0.0 copy-start.4
  4.4 0.0 copy-start.5
  4.5 0.8 copy.60.query_ref
  5.3 0.0 copy-done.3
  5.3 0.1 copy.58
  5.4 0.0 copy-done.8
  5.4 0.1 fusion.9
  5.5 0.3 subtract_convert_fusion.1
  5.8 0.1 copy.59
  5.9 1.2 reduce-window.6
  7.1 0.1 slice.40
  7.2 0.1 copy.54
  7.4 0.1 copy.55
  7.5 0.1 add_bitcast_fusion
  7.6 0.1 reduce_sum.60
  7.7 0.1 copy.56
  7.8 0.0 copy-done.6
  7.8 0.1 convert_reduce_fusion
  7.9 0.0 copy-done.2
  7.9 0.2 fusion.2
  8.1 0.0 copy-done.4
  8.1 0.7 pad_maximum_fusion.1.pair_ref
  8.8 0.0 copy-done.5
  8.8 1.8 %convolution_convert_fusion = bf16[384,2048]{1,0:T(8,128)(2,1)} fusion(bf16[128,2048]{1,0:T(8,128)(2,1)S(1)} %copy-done.2, f32[2048]{0:T(1024)S(1)} %copy-done.5, f32[128]{0:T(128)S(1)} %add_rsqrt_fusion.2, s32[128,384]{1,0:T(8,128)S(1)} %convert_reduce_fusion), kind=kOutput, calls=%fused_computation | convolution fusion | flops 203210752 | bytes 2302464 | tf_op jit(solution)/shard_map/re,rd->ed/dot_general | solution.py:428
  10.6 114.5 %shard_map.140 = (bf16[4,96,2048]{2,1,0:T(8,128)(2,1)}, bf16[192,512]{1,0:T(8,128)(2,1)}) custom-call(bf16[4,96,2048]{2,1,0:T(8,128)(2,1)} %bitcast.49, bf16[2048,512]{1,0:T(8,128)(2,1)} %bitcast.52, bf16[2048,512]{1,0:T(8,128)(2,1)} %bitcast.53, bf16[512,2048]{1,0:T(8,128)(2,1)} %bitcast.54, bf16[192,512]{1,0:T(8,128)(2,1)} %copy.60.query_ref, ...), custom_call_target="tpu_custom_call" | custom-call | tf_op jit(solution)/shard_map/pallas_call | solution.py:330
  125.1 0.0 copy-done
  125.1 0.0 copy-start.7
  125.1 2.4 %convolution_convert_fusion.1 = bf16[192,2048]{1,0:T(8,128)(2,1)} fusion(bf16[192,512]{1,0:T(8,128)(2,1)} %get-tuple-element.4, bf16[512,2048]{1,0:T(8,128)(2,1)S(1)} %copy-done), kind=kOutput, calls=%fused_computation.1 | convolution fusion | flops 403046400 | bytes 3080192 | tf_op jit(solution)/shard_map/dot_general | solution.py:458
  127.5 3.5 %all-to-all-start = ((bf16[4,48,2048]{2,1,0:T(8,128)(2,1)}), bf16[4,48,2048]{2,1,0:T(8,128)(2,1)S(1)}, u32[]{:S(2)}, u32[]{:S(2)}) async-start(bf16[4,48,2048]{2,1,0:T(8,128)(2,1)} %bitcast.50), calls=%async_computation | async-start | bytes 1572864 | tf_op jit(solution)/shard_map/all_to_all | solution.py:461
  131.0 0.0 copy-start.1
  131.1 0.0 copy-done.7
  131.1 2.0 %convolution_multiply_fusion.1 = f32[128,2048]{1,0:T(8,128)S(1)} fusion(bf16[384,2048]{1,0:T(8,128)(2,1)} %bitcast.47, f32[128]{0:T(128)S(1)} %bitcast.59, s32[128]{0:T(128)S(1)} %get-tuple-element.19), kind=kOutput, calls=%fused_computation.4 | convolution fusion | flops 201637888 | bytes 2622464 | tf_op jit(solution)/shard_map/dot_general | solution.py:473
  133.1 0.0 copy-done.1
  133.1 1.3 fusion.1
  134.4 8.2 %all-to-all-done = bf16[4,48,2048]{2,1,0:T(8,128)(2,1)S(1)} async-done(((bf16[4,48,2048]{2,1,0:T(8,128)(2,1)}), bf16[4,48,2048]{2,1,0:T(8,128)(2,1)S(1)}, u32[]{:S(2)}, u32[]{:S(2)}) %all-to-all-start) | async-done | bytes 786464 | tf_op jit(solution)/shard_map/all_to_all | solution.py:461
  142.6 0.8 reduce_sum.65
  (15 shorter events, 0.2 us)
Async XLA Ops:
  0.6 124.5 %copy-start = (bf16[512,2048]{1,0:T(8,128)(2,1)S(1)}, bf16[512,2048]{1,0:T(8,128)(2,1)}, u32[]{:S(2)}) copy-start(bf16[512,2048]{1,0:T(8,128)(2,1)} %param.18) | copy-start | bytes 6291460
  3.0 2.2 %copy-start.3 = (bf16[192,128]{1,0:T(8,128)(2,1)S(1)}, bf16[192,128]{1,0:T(8,128)(2,1)}, u32[]{:S(2)}) copy-start(bf16[192,128]{1,0:T(8,128)(2,1)} %param.14) | copy-start | bytes 147460
  3.9 1.5 %copy-start.8 = (f32[128]{0:T(128)S(1)}, f32[128]{0:T(128)}, u32[]{:S(2)}) copy-start(f32[128]{0:T(128)} %param.17) | copy-start | bytes 1540
  4.3 3.5 %copy-start.6 = (s32[128,2]{0,1:T(2,128)S(1)}, s32[128,2]{0,1:T(2,128)}, u32[]{:S(2)}) copy-start(s32[128,2]{0,1:T(2,128)} %param.21) | copy-start | bytes 3076
  4.3 3.6 %copy-start.2 = (bf16[128,2048]{1,0:T(8,128)(2,1)S(1)}, bf16[128,2048]{1,0:T(8,128)(2,1)}, u32[]{:S(2)}) copy-start(bf16[128,2048]{1,0:T(8,128)(2,1)} %param.19) | copy-start | bytes 1572868
  4.4 3.7 %copy-start.4 = (bf16[192,128]{1,0:T(8,128)(2,1)S(1)}, bf16[192,128]{1,0:T(8,128)(2,1)}, u32[]{:S(2)}) copy-start(bf16[192,128]{1,0:T(8,128)(2,1)} %param.15) | copy-start | bytes 147460
  4.4 4.4 %copy-start.5 = (f32[2048]{0:T(1024)S(1)}, f32[2048]{0:T(1024)}, u32[]{:S(2)}) copy-start(f32[2048]{0:T(1024)} %param.20) | copy-start | bytes 24580
  125.1 5.9 %copy-start.7 = (f32[128,2]{0,1:T(2,128)S(1)}, f32[128,2]{0,1:T(2,128)}, u32[]{:S(2)}) copy-start(f32[128,2]{0,1:T(2,128)} %param.22) | copy-start | bytes 3076
  127.5 15.1 %all-to-all-start = ((bf16[4,48,2048]{2,1,0:T(8,128)(2,1)}), bf16[4,48,2048]{2,1,0:T(8,128)(2,1)S(1)}, u32[]{:S(2)}, u32[]{:S(2)}) async-start(bf16[4,48,2048]{2,1,0:T(8,128)(2,1)} %bitcast.50), calls=%async_computation | async-start | bytes 1572864 | tf_op jit(solution)/shard_map/all_to_all | solution.py:461
  131.0 2.1 %copy-start.1 = (bf16[4,96,2048]{2,1,0:T(8,128)(2,1)S(1)}, bf16[4,96,2048]{2,1,0:T(8,128)(2,1)}, u32[]{:S(2)}) copy-start(bf16[4,96,2048]{2,1,0:T(8,128)(2,1)} %get-tuple-element.5) | copy-start | bytes 4718596
where the time goes:
time: 144 us; the launch traced here: 143 us
  Pallas kernels  115 us (80%)
  waiting for transfers between devices  8.23 us (6%)
  matrix products  7.51 us (5%)
  local copies, waits for them, and re-layouts  4.56 us (3%)
  other arithmetic  4.23 us (3%)
  starting transfers between devices  3.49 us (2%)
    pallas_call x1, Pallas kernels, exchange(): pl.pallas_call(functools.partial(exchange_kernel, steps), out_shape=(jax....  115 us
    all_to_all x1, waiting for transfers between devices, both_halves(): lax.all_to_all(head_partial.reshape(lanes, -1, head_partial.shape[1]), 't...  8.23 us
    all_to_all x1, starting transfers between devices, both_halves(): lax.all_to_all(head_partial.reshape(lanes, -1, head_partial.shape[1]), 't...  3.49 us
    dot_general x2, matrix products, both_halves(): jnp.dot((picks[:, k:k + 1] == jnp.arange(experts_all * capacity, dtype=jn...  3.3 us
  transfers between devices with their start and end apart: 1, of which 1 were waited for; matrix products, arithmetic and copies ran while one was open for 2% of the time, Pallas kernels for 0%

commit v1 on v0

v1 whole, which is shorter than its diff:
```python
import functools
import math

import jax
import jax.numpy as jnp
import numpy as np
from jax import lax
from jax.experimental import pallas as pl
from jax.experimental.pallas import tpu as pltpu
from jax.sharding import PartitionSpec as P

GRID_W = 64


MESH = pl.DeviceIdType.MESH
EPS = 1e-06
THETA = 10000.0


def head_norm(vectors, gain):
    return vectors * lax.rsqrt(jnp.mean(vectors * vectors, axis=-1, keepdims=True) + EPS) * gain


def rotate_grid(vectors, token_positions):
    length, heads, head_dim = vectors.shape
    quarter = head_dim // 4
    freqs = 1.0 / THETA ** (jnp.arange(quarter, dtype=jnp.float32) * 4.0 / head_dim)
    grid_row = (token_positions // GRID_W).astype(jnp.float32)
    grid_col = (token_positions % GRID_W).astype(jnp.float32)
    angles = jnp.stack([grid_row[:, None] * freqs, grid_col[:, None] * freqs], axis=1)
    cosine = jnp.cos(angles)[:, None]
    sine = jnp.sin(angles)[:, None]
    halves = vectors.reshape(length, heads, 2, 2, quarter)
    first = halves[..., 0, :]
    second = halves[..., 1, :]
    turned = jnp.stack([first * cosine - second * sine, second * cosine + first * sine], axis=-2)
    return turned.reshape(length, heads, head_dim)


def prepare_inputs(raw_rows, gain, heads, token_positions):
    length = raw_rows.shape[0]
    head_dim = gain.shape[0]
    vectors = raw_rows.astype(jnp.float32).reshape(length, heads, head_dim)
    return rotate_grid(head_norm(vectors, gain), token_positions).astype(jnp.bfloat16)


def mixer_prepare(query_rows, projected_keys, projected_values, query_gain, key_norm_gain):
    length = query_rows.shape[0]
    head_dim = query_gain.shape[0]
    kv_heads = projected_keys.shape[1] // head_dim
    q_heads = query_rows.shape[1] // head_dim
    token_positions = lax.axis_index("ep") * length + jnp.arange(length, dtype=jnp.int32)
    query_matrix = prepare_inputs(query_rows, query_gain, q_heads, token_positions).reshape(
        length, q_heads * head_dim
    )
    keys_turned = prepare_inputs(projected_keys, key_norm_gain, kv_heads, token_positions).reshape(
        length, kv_heads * head_dim
    )
    return query_matrix, jnp.concatenate([keys_turned, projected_values], axis=1)


def attend_plain(query_matrix, own_pair, head_dim):
    length = query_matrix.shape[0]
    kv_heads = own_pair.shape[1] // (2 * head_dim)
    q_heads = query_matrix.shape[1] // head_dim
    queries_per_group = q_heads // kv_heads
    query_matrix = query_matrix.reshape(length, kv_heads, queries_per_group, head_dim)
    score_scale = head_dim ** (-0.5)
    initial = (
        jnp.full((kv_heads, queries_per_group, length), -1e30, jnp.float32),
        jnp.zeros((kv_heads, queries_per_group, length), jnp.float32),
        jnp.zeros((length, kv_heads, queries_per_group, head_dim), jnp.float32),
    )
    width = kv_heads * head_dim
    pair = lax.all_gather(own_pair, "ep", axis=0, tiled=True)
    key_piece = pair[:, :width]
    value_piece = pair[:, width:]
    piece_rows = key_piece.shape[0]
    step_rows = math.gcd(piece_rows, 1024)

    def one_block(block_index, running):
        run_max, run_sum, run_acc = running
        offset = block_index * step_rows
        key_block = lax.dynamic_slice_in_dim(key_piece, offset, step_rows, 0).reshape(
            step_rows, kv_heads, head_dim
        )
        value_block = lax.dynamic_slice_in_dim(value_piece, offset, step_rows, 0).reshape(
            step_rows, kv_heads, head_dim
        )
        scores = (
            jnp.einsum(
                "tkgd,skd->kgts", query_matrix, key_block, preferred_element_type=jnp.float32
            )
            * score_scale
        )
        new_max = jnp.maximum(run_max, jnp.max(scores, axis=-1))
        factor = jnp.exp(run_max - new_max)
        weights = jnp.exp(scores - new_max[..., None])
        run_sum = run_sum * factor + jnp.sum(weights, axis=-1)
        update = jnp.einsum(
            "kgts,skd->tkgd",
            weights.astype(jnp.bfloat16),
            value_block,
            preferred_element_type=jnp.float32,
        )
        run_acc = run_acc * jnp.transpose(factor, (2, 0, 1))[..., None] + update
        return (new_max, run_sum, run_acc)

    run_max, run_sum, run_acc = lax.fori_loop(0, piece_rows // step_rows, one_block, initial)
    return (
        (run_acc / jnp.transpose(run_sum, (2, 0, 1))[..., None])
        .astype(jnp.bfloat16)
        .reshape(length, q_heads * head_dim)
    )


def flip(index, bits):
    result, place = 0, 1
    for _ in range(8):
        mine = (index // place) % 2
        result = result + place * ((1 - mine) if bits & place else mine)
        place *= 2
    return result


def exchange_plain(outgoing, gate_proj, up_proj, down_proj):
    rows_in = lax.all_gather(
        lax.all_to_all(outgoing, "ep", split_axis=0, concat_axis=0, tiled=True),
        "tp",
        axis=0,
        tiled=True,
    )
    gate_out = jnp.einsum("secd,edf->secf", rows_in, gate_proj, preferred_element_type=jnp.float32)
    up_out = jnp.einsum("secd,edf->secf", rows_in, up_proj, preferred_element_type=jnp.float32)
    active = (jax.nn.silu(gate_out) * up_out).astype(jnp.bfloat16)
    summed = lax.psum_scatter(
        jnp.einsum("secf,efd->secd", active, down_proj, preferred_element_type=jnp.float32).astype(
            jnp.bfloat16
        ),
        "tp",
        scatter_dimension=0,
        tiled=True,
    )
    return lax.all_to_all(summed, "ep", split_axis=0, concat_axis=0, tiled=True)


def plain_halves(
    query_rows,
    projected_keys,
    projected_values,
    query_gain,
    key_norm_gain,
    out_proj,
    mix_tokens,
    norm_gain,
    expert_ids,
    expert_score,
    gate_proj,
    up_proj,
    down_proj,
):
    length, model_dim = mix_tokens.shape
    top_count = expert_ids.shape[1]
    local_experts = gate_proj.shape[0]
    expert_axis = lax.axis_size("ep")
    experts_all = expert_axis * local_experts
    capacity = length * top_count * 3 // (2 * experts_all)
    values_b = mix_tokens.astype(jnp.float32)
    normed = (
        values_b
        * lax.rsqrt(jnp.mean(values_b * values_b, axis=-1, keepdims=True) + EPS)
        * norm_gain
    ).astype(jnp.bfloat16)
    flat = expert_ids.reshape(length * top_count)
    onehot = (flat[:, None] == jnp.arange(experts_all, dtype=jnp.int32)).astype(jnp.int32)
    slots = jnp.sum((jnp.cumsum(onehot, axis=0) - onehot) * onehot, axis=1)
    target = flat * capacity + slots
    placed = (target[:, None] == jnp.arange(experts_all * capacity, dtype=jnp.int32)).astype(
        jnp.int32
    )
    placed = jnp.sum(placed.reshape(length, top_count, experts_all * capacity), axis=1).astype(
        jnp.bfloat16
    )
    outgoing = jnp.einsum("re,rd->ed", placed, normed, preferred_element_type=jnp.float32).astype(
        jnp.bfloat16
    )
    outgoing = outgoing.reshape(expert_axis, local_experts, capacity, model_dim)
    lanes = lax.axis_size("tp")
    head_dim = query_gain.shape[0]
    queries, pair = mixer_prepare(
        query_rows, projected_keys, projected_values, query_gain, key_norm_gain
    )
    heads_out = attend_plain(queries, pair, head_dim)
    returned = exchange_plain(outgoing, gate_proj, up_proj, down_proj)
    head_partial = jnp.dot(heads_out, out_proj, preferred_element_type=jnp.float32).astype(
        jnp.bfloat16
    )
    pieces = lax.all_to_all(
        head_partial.reshape(lanes, -1, head_partial.shape[1]),
        "tp",
        split_axis=0,
        concat_axis=0,
        tiled=True,
    )
    mixed_rows = jnp.sum(pieces.astype(jnp.float32), axis=0).astype(jnp.bfloat16)
    results = returned.reshape(experts_all * capacity, model_dim)
    first_weight = jax.nn.sigmoid(expert_score[:, 0] - expert_score[:, 1])
    picks = target.reshape(length, top_count)
    chosen = [
        jnp.dot(
            (picks[:, k : k + 1] == jnp.arange(experts_all * capacity, dtype=jnp.int32)).astype(
                jnp.bfloat16
            ),
            results,
            preferred_element_type=jnp.float32,
        )
        for k in range(2)
    ]
    combined = first_weight[:, None] * chosen[0] + (1.0 - first_weight)[:, None] * chosen[1]
    return (mixed_rows, combined.astype(jnp.bfloat16))


ORDER = (
    "A10", "A11", "A31", "B31", "B11", "A30", "C31", "KV0",
    "D31", "B00", "A20", "A21", "KV1", "B30", "C00", "C30",
    "D30", "B10", "E31", "KV2", "D00", "B21", "C21", "E30",
    "D21", "B20", "B01", "ATT0", "C10", "C01", "D10", "C20",
    "ATT1", "E00", "E21", "D20", "ATT2", "ATT3", "E10", "D01",
    "C11", "D11", "E20", "E01", "CMB0", "OUTP", "MX0", "E11",
    "CMB2", "CMB3", "MX1", "CMB1",
)
VMEM_LIMIT = 58 * 1024 * 1024
SENDS = ((1, 1), (1, 0), (3, 1), (3, 0), (2, 0), (2, 1))


def fused_kernel(
    steps,
    order,
    tokens_ref,
    ids_ref,
    score_ref,
    ngain_ref,
    gate_hbm,
    up_hbm,
    down_hbm,
    proj_hbm,
    query_hbm,
    key_hbm,
    value_hbm,
    qgain_ref,
    kgain_ref,
    cos_hbm,
    sin_hbm,
    mixed_ref,
    expert_ref,
    gate_ref,
    up_ref,
    down_ref,
    proj_ref,
    query_ref,
    keyraw_ref,
    cos_ref,
    sin_ref,
    tok_ref,
    norm_ref,
    outb,
    rows,
    act,
    part,
    from_core,
    to_x,
    from_x,
    total,
    back,
    acc,
    lut,
    kv,
    heads_ref,
    pm,
    fc,
    to_xm,
    from_xm,
    hsem,
    zs,
    zr,
    xs,
    xr,
    cs,
    cr,
    ps,
    pr,
    qs,
    qr,
    bs,
    br,
    ks,
    kr,
    ms,
    mr,
):
    me = lax.axis_index("ep")
    lane = lax.axis_index("tp")
    peers = [flip(me, k) for k in range(steps)]
    core, across = flip(lane, 1), flip(lane, 2)
    cap, width = outb.shape[1], outb.shape[2]
    half = cap // 2
    hidden = gate_ref.shape[1]
    length = query_ref.shape[0]
    dim = keyraw_ref.shape[1]
    count = tok_ref.shape[0]
    tile = math.gcd(hidden, 256)
    tile_out = math.gcd(width, 512)
    f32, b16 = jnp.float32, jnp.bfloat16

    offset = pl.multiple_of(me * length, 16)
    loads = [
        pltpu.make_async_copy(s, d, hsem.at[i])
        for i, (s, d) in enumerate(
            [
                (tokens_ref, tok_ref),
                (key_hbm, keyraw_ref),
                (value_hbm, kv.at[0, 1]),
                (cos_hbm.at[pl.ds(offset, length)], cos_ref),
                (sin_hbm.at[pl.ds(offset, length)], sin_ref),
                (query_hbm, query_ref),
                (gate_hbm, gate_ref),
                (up_hbm, up_ref),
                (down_hbm, down_ref),
                (proj_hbm, proj_ref),
            ]
        )
    ]
    for load in loads:
        load.start()

    barrier = pltpu.get_barrier_semaphore()
    friends = [{"ep": peers[k], "tp": lane} for k in range(1, steps)]
    friends += [{"ep": me, "tp": core}, {"ep": me, "tp": across}]
    for friend in friends:
        pl.semaphore_signal(barrier, inc=1, device_id=friend, device_id_type=MESH)

    def remote(src, dst, send, recv, ep_to, tp_to):
        return pltpu.make_async_remote_copy(
            src_ref=src,
            dst_ref=dst,
            send_sem=send,
            recv_sem=recv,
            device_id={"ep": ep_to, "tp": tp_to},
            device_id_type=MESH,
        )

    def piece(h):
        return pl.ds(h * half, half)

    units = [(k, h) for k in range(steps) for h in range(2)]
    z_in, x_in, c_in, c_out, x_out, z_out = {}, {}, {}, {}, {}, {}
    for k, h in units:
        n = 2 * k + h
        if k:
            z_in[k, h] = remote(
                outb.at[k, piece(h)], rows.at[k, h, 0], zs.at[n], zr.at[n], peers[k], lane
            )
            z_out[k, h] = remote(
                total.at[k, h], back.at[k, piece(h)], bs.at[n], br.at[n], peers[k], lane
            )
        x_in[k, h] = remote(rows.at[k, h, 0], rows.at[k, h, 1], xs.at[n], xr.at[n], me, across)
        c_in[k, h] = remote(
            rows.at[k, h, pl.ds(0, 2)], rows.at[k, h, pl.ds(2, 2)], cs.at[n], cr.at[n], me, core
        )
        c_out[k, h] = remote(
            part.at[k, h, pl.ds(2, 2)], from_core.at[k, h], ps.at[n], pr.at[n], me, core
        )
        x_out[k, h] = remote(to_x.at[k, h], from_x.at[k, h], qs.at[n], qr.at[n], me, across)
    kv_near = remote(kv.at[0], kv.at[1], ks.at[0], kr.at[0], peers[1], lane)
    kv_mid = remote(kv.at[pl.ds(0, 2)], kv.at[pl.ds(2, 2)], ks.at[1], kr.at[1], peers[3], lane)
    kv_far = remote(kv.at[pl.ds(2, 2)], kv.at[pl.ds(2, 2)], ks.at[2], kr.at[2], peers[1], lane)
    inner = (me == 1) | (me == 2)
    m_core = [
        remote(pm.at[core], fc.at[0], ms.at[0], mr.at[0], me, core),
        remote(pm.at[flip(core, 2)], fc.at[1], ms.at[1], mr.at[1], me, core),
    ]
    m_x = remote(to_xm, from_xm, ms.at[2], mr.at[2], me, across)

    token_row = lax.broadcasted_iota(jnp.int32, (count, count), 0)
    token_col = lax.broadcasted_iota(jnp.int32, (count, count), 1)
    earlier = (token_row < token_col).astype(b16)
    first, second = ids_ref[0:1, :], ids_ref[1:2, :]
    weight = 1.0 / (1.0 + jnp.exp(score_ref[1:2, :] - score_ref[0:1, :]))
    table_row = lax.broadcasted_iota(jnp.int32, (8, count), 0)
    named = jnp.zeros((8, count), f32)
    scale = jnp.zeros((8, count), f32)
    for k in range(steps):
        one, two = first == peers[k], second == peers[k]
        here = jnp.where(one | two, 1.0, 0.0)
        named = jnp.where(table_row == k, here, named)
        value = jnp.where(one, weight, 0.0) + jnp.where(two, 1.0 - weight, 0.0)
        scale = jnp.where(table_row == k, value, scale)
    rank = jnp.dot(named.astype(b16), earlier, preferred_element_type=f32)
    place = jnp.where(named > 0.5, rank, -1.0)
    rest = jnp.zeros((count - 16, count), f32)
    lut[...] = jnp.transpose(jnp.concatenate([place, scale, rest], axis=0))

    loads[0].wait()
    values = tok_ref[...].astype(f32)
    norm_ref[...] = (
        values
        * lax.rsqrt(jnp.mean(values * values, axis=-1, keepdims=True) + EPS)
        * ngain_ref[...]
    ).astype(b16)

    slot = lax.broadcasted_iota(jnp.int32, (cap, count), 0).astype(f32)

    def dispatch(k):
        chosen = (slot == place[k : k + 1, :]).astype(b16)
        picked = jnp.dot(chosen, norm_ref[...], preferred_element_type=f32).astype(b16)
        if k:
            outb[k] = picked
        else:
            rows[0, 0, 0] = picked[:half]
            rows[0, 1, 0] = picked[half:]

    sent = {SENDS[0][0], 0}
    dispatch(SENDS[0][0])
    dispatch(0)
    pl.semaphore_wait(barrier, len(friends))
    z_in[SENDS[0]].start()
    for h in range(2):
        x_in[0, h].start()
    for k, h in SENDS[1:]:
        if k not in sent:
            sent.add(k)
            dispatch(k)
        z_in[k, h].start()

    turn_lane = lax.broadcasted_iota(jnp.int32, (length, dim), 1)
    leading = (turn_lane // (dim // 4)) % 2 == 0

    def turned(raw, gain):
        vectors = raw.astype(f32)
        vectors = (
            vectors
            * lax.rsqrt(jnp.mean(vectors * vectors, axis=-1, keepdims=True) + EPS)
            * gain[...]
        )
        other = jnp.where(
            leading,
            pltpu.roll(vectors, dim - dim // 4, 1),
            pltpu.roll(vectors, dim // 4, 1),
        )
        return (vectors * cos_ref[...] + other * sin_ref[...]).astype(b16)

    def stage_a(k, h):
        z_in[k, h].wait_recv()
        x_in[k, h].start()

    def stage_b(k, h):
        x_in[k, h].wait_recv()
        c_in[k, h].start()

    def stage_c(k, h):
        c_in[k, h].wait_recv()

        @pl.loop(0, hidden // tile)
        def _(i):
            cols = pl.ds(pl.multiple_of(i * tile, tile), tile)
            block = rows[k, h].reshape(4 * half, width)
            gate = jnp.dot(block, gate_ref[:, cols], preferred_element_type=f32)
            up = jnp.dot(block, up_ref[:, cols], preferred_element_type=f32)
            act[:, cols] = (gate / (1.0 + jnp.exp(-gate)) * up).astype(b16)

        @pl.loop(0, width // tile_out)
        def _(i):
            cols = pl.ds(pl.multiple_of(i * tile_out, tile_out), tile_out)
            summed = jnp.dot(act[...], down_ref[:, cols], preferred_element_type=f32)
            part[k, h, :, :, cols] = summed.astype(b16).reshape(4, half, tile_out)

        c_out[k, h].start()

    def stage_d(k, h):
        c_out[k, h].wait_recv()
        to_x[k, h] = (part[k, h, 1].astype(f32) + from_core[k, h, 1].astype(f32)).astype(b16)
        x_out[k, h].start()

    def stage_e(k, h):
        x_out[k, h].wait_recv()
        summed = (
            part[k, h, 0].astype(f32) + from_core[k, h, 0].astype(f32) + from_x[k, h].astype(f32)
        ).astype(b16)
        if k == 0:
            back[0, piece(h)] = summed
        else:
            total[k, h] = summed
            z_out[k, h].start()

    def stage_kv0():
        loads[1].wait()
        loads[2].wait()
        loads[3].wait()
        loads[4].wait()
        kv[0, 0] = turned(keyraw_ref[...], kgain_ref)
        kv_near.start()

    def stage_kv1():
        kv_near.wait_recv()

        @pl.when(inner)
        def _():
            kv_mid.start()

    def stage_kv2():
        @pl.when(inner)
        def _():
            kv_mid.wait_recv()
            kv_far.start()

    def stage_att(head):
        if head == 0:
            loads[5].wait()

            @pl.when(jnp.logical_not(inner))
            def _():
                kv_far.wait_recv()

        cols = slice(head * dim, (head + 1) * dim)
        held = steps * length
        queries = turned(query_ref[:, cols], qgain_ref)
        keys = kv[:, 0].reshape(held, dim)
        scores = (
            lax.dot_general(
                queries, keys, (((1,), (1,)), ((), ())), preferred_element_type=f32
            )
            * dim ** (-0.5)
        )
        probs = jnp.exp(scores - jnp.max(scores, axis=-1, keepdims=True))
        amount = jnp.sum(probs, axis=-1, keepdims=True)
        summed = jnp.dot(
            probs.astype(b16), kv[:, 1].reshape(held, dim), preferred_element_type=f32
        )
        heads_ref[:, cols] = (summed / amount).astype(b16)

    def stage_outp():
        loads[9].wait()

        @pl.loop(0, width // tile_out)
        def _(i):
            cols = pl.ds(pl.multiple_of(i * tile_out, tile_out), tile_out)
            summed = jnp.dot(heads_ref[...], proj_ref[:, cols], preferred_element_type=f32)
            pm[:, :, cols] = summed.astype(b16).reshape(4, length // 4, tile_out)

        for copy in m_core:
            copy.start()

    def stage_mx(step):
        if step == 0:
            for copy in m_core:
                copy.wait_recv()
            to_xm[...] = (pm[across].astype(f32) + fc[1].astype(f32)).astype(b16)
            m_x.start()
        else:
            m_x.wait_recv()
            mixed_ref[...] = (
                pm[lane].astype(f32) + fc[0].astype(f32) + from_xm[...].astype(f32)
            ).astype(b16)

    combined = []

    def stage_cmb(k):
        if k > 0:
            for h in range(2):
                z_out[k, h].wait_recv()
        spot = lax.broadcasted_iota(jnp.int32, (count, cap), 1).astype(f32)
        chosen = (spot == lut[:, k : k + 1]).astype(b16)
        scaled = lut[:, 8 + k : 9 + k]
        opening, closing = not combined, len(combined) == steps - 1
        combined.append(k)

        @pl.loop(0, width // tile_out)
        def _(i):
            cols = pl.ds(pl.multiple_of(i * tile_out, tile_out), tile_out)
            found = scaled * jnp.dot(chosen, back[k, :, cols], preferred_element_type=f32)
            if not opening:
                found = acc[:, cols] + found
            if closing:
                expert_ref[:, cols] = found.astype(b16)
            else:
                acc[:, cols] = found

    stages = {"A": stage_a, "B": stage_b, "C": stage_c, "D": stage_d, "E": stage_e}
    loaded = False
    for name in order:
        if name[0] == "C" and name[1] != "M" and not loaded:
            loaded = True
            for n in (6, 7, 8):
                loads[n].wait()
        if name.startswith("KV"):
            (stage_kv0, stage_kv1, stage_kv2)[int(name[2])]()
        elif name.startswith("ATT"):
            stage_att(int(name[3]))
        elif name == "OUTP":
            stage_outp()
        elif name.startswith("MX"):
            stage_mx(int(name[2]))
        elif name.startswith("CMB"):
            stage_cmb(int(name[3]))
        else:
            stages[name[0]](int(name[1]), int(name[2]))

    for unit in units:
        for table in (z_in, x_in, c_in, c_out, x_out, z_out):
            if unit in table:
                table[unit].wait_send()
    kv_near.wait_send()

    @pl.when(inner)
    def _():
        kv_mid.wait_send()
        kv_far.wait_send()

    for copy in m_core:
        copy.wait_send()
    m_x.wait_send()


def deliver_kernel(mixed_in, expert_in, mixed_out, expert_out, mixed_held, expert_held, sems):
    pairs = []
    for source, held, target, pieces in (
        (expert_in, expert_held, expert_out, 4),
        (mixed_in, mixed_held, mixed_out, 1),
    ):
        size = source.shape[0] // pieces
        for n in range(pieces):
            spot = pl.ds(n * size, size)
            at = len(pairs)
            pairs.append(
                (
                    pltpu.make_async_copy(source.at[spot], held.at[spot], sems.at[0, at]),
                    pltpu.make_async_copy(held.at[spot], target.at[spot], sems.at[1, at]),
                )
            )
    for fetch, _ in pairs:
        fetch.start()
    for fetch, store in pairs:
        fetch.wait()
        store.start()
    for _, store in pairs:
        store.wait()


def turn_tables(held, dim):
    quarter = dim // 4
    freqs = 1.0 / THETA ** (np.arange(quarter) * 4.0 / dim)
    spots = np.arange(held)
    tables = []
    for place in (spots // GRID_W, spots % GRID_W):
        angles = place[:, None] * freqs
        tables.append((np.cos(angles), np.sin(angles)))
    cosine = np.concatenate([tables[0][0]] * 2 + [tables[1][0]] * 2, axis=1)
    sine = np.concatenate(
        [-tables[0][1], tables[0][1], -tables[1][1], tables[1][1]], axis=1
    )
    return jnp.asarray(cosine, jnp.float32), jnp.asarray(sine, jnp.float32)


def fused(
    query_rows,
    projected_keys,
    projected_values,
    query_gain,
    key_norm_gain,
    out_proj,
    mix_tokens,
    norm_gain,
    expert_ids,
    expert_score,
    gate_proj,
    up_proj,
    down_proj,
):
    steps, lanes = lax.axis_size("ep"), lax.axis_size("tp")
    count, width = mix_tokens.shape
    cap = count * expert_ids.shape[1] * 3 // (2 * steps)
    half = cap // 2
    hidden = gate_proj.shape[2]
    length, dim = projected_keys.shape
    kind = jnp.bfloat16
    cosine, sine = turn_tables(steps * length, dim)
    vmem = pl.BlockSpec(memory_space=pltpu.VMEM)
    anywhere = pl.BlockSpec(memory_space=pltpu.HBM)
    units = 2 * steps
    mixed, expert = pl.pallas_call(
        functools.partial(fused_kernel, steps, ORDER),
        out_shape=(
            jax.ShapeDtypeStruct((length // lanes, width), kind),
            jax.ShapeDtypeStruct((count, width), kind),
        ),
        in_specs=[anywhere]
        + [vmem] * 3
        + [anywhere] * 7
        + [vmem] * 2
        + [anywhere] * 2,
        out_specs=(vmem, vmem),
        scratch_shapes=[
            pltpu.VMEM((width, hidden), kind),
            pltpu.VMEM((width, hidden), kind),
            pltpu.VMEM((hidden, width), kind),
            pltpu.VMEM(out_proj.shape, kind),
            pltpu.VMEM(query_rows.shape, kind),
            pltpu.VMEM((length, dim), kind),
            pltpu.VMEM((length, dim), jnp.float32),
            pltpu.VMEM((length, dim), jnp.float32),
            pltpu.VMEM((count, width), kind),
            pltpu.VMEM((count, width), kind),
            pltpu.VMEM((steps, cap, width), kind),
            pltpu.VMEM((steps, 2, 4, half, width), kind),
            pltpu.VMEM((4 * half, hidden), kind),
            pltpu.VMEM((steps, 2, 4, half, width), kind),
            pltpu.VMEM((steps, 2, 2, half, width), kind),
            pltpu.VMEM((steps, 2, half, width), kind),
            pltpu.VMEM((steps, 2, half, width), kind),
            pltpu.VMEM((steps, 2, half, width), kind),
            pltpu.VMEM((steps, cap, width), kind),
            pltpu.VMEM((count, width), jnp.float32),
            pltpu.VMEM((count, count), jnp.float32),
            pltpu.VMEM((steps, 2, length, dim), kind),
            pltpu.VMEM(query_rows.shape, kind),
            pltpu.VMEM((lanes, length // lanes, width), kind),
            pltpu.VMEM((2, length // lanes, width), kind),
            pltpu.VMEM((length // lanes, width), kind),
            pltpu.VMEM((length // lanes, width), kind),
            pltpu.SemaphoreType.DMA((10,)),
        ]
        + [pltpu.SemaphoreType.DMA((units,))] * 12
        + [pltpu.SemaphoreType.DMA((3,))] * 4,
        compiler_params=pltpu.CompilerParams(
            collective_id=0, has_side_effects=True, vmem_limit_bytes=VMEM_LIMIT
        ),
    )(
        mix_tokens,
        expert_ids.T,
        expert_score.T,
        norm_gain.reshape(1, width),
        gate_proj.reshape(gate_proj.shape[1:]),
        up_proj.reshape(up_proj.shape[1:]),
        down_proj.reshape(down_proj.shape[1:]),
        out_proj,
        query_rows,
        projected_keys,
        projected_values,
        query_gain.reshape(1, dim),
        key_norm_gain.reshape(1, dim),
        cosine,
        sine,
    )
    return pl.pallas_call(
        deliver_kernel,
        out_shape=(
            jax.ShapeDtypeStruct(mixed.shape, kind),
            jax.ShapeDtypeStruct(expert.shape, kind),
        ),
        in_specs=[anywhere] * 2,
        out_specs=(anywhere, anywhere),
        scratch_shapes=[
            pltpu.VMEM(mixed.shape, kind),
            pltpu.VMEM(expert.shape, kind),
            pltpu.SemaphoreType.DMA((2, 5)),
        ],
    )(mixed, expert)


def fits_fused(query_rows, projected_keys, query_gain, mix_tokens, expert_ids, gate_proj):
    steps, lanes = lax.axis_size("ep"), lax.axis_size("tp")
    count, width = mix_tokens.shape
    length, dim = projected_keys.shape
    local_experts, _, hidden = gate_proj.shape
    cap = count * expert_ids.shape[1] * 3 // (2 * steps)
    blocks = 20 * steps * cap * width * 2 + 4 * width * hidden * 2
    return (
        lanes == 4
        and steps == 4
        and local_experts == 1
        and expert_ids.shape[1] == 2
        and dim == query_gain.shape[0]
        and dim % 128 == 0
        and length % 64 == 0
        and length <= 256
        and count == 128
        and cap % 32 == 0
        and blocks < 48 * 1024 * 1024
    )


def local(
    query_rows,
    projected_keys,
    projected_values,
    query_gain,
    key_norm_gain,
    out_proj,
    mix_tokens,
    norm_gain,
    expert_ids,
    expert_score,
    gate_proj,
    up_proj,
    down_proj,
):
    simple = fits_fused(
        query_rows, projected_keys, query_gain, mix_tokens, expert_ids, gate_proj
    )
    return (fused if simple else plain_halves)(
        query_rows,
        projected_keys,
        projected_values,
        query_gain,
        key_norm_gain,
        out_proj,
        mix_tokens,
        norm_gain,
        expert_ids,
        expert_score,
        gate_proj,
        up_proj,
        down_proj,
    )


def solution(mesh):
    in_specs = (
        P(("grp", "ep"), "tp"),
        P(("grp", "ep"), "tp"),
        P(("grp", "ep"), "tp"),
        P(),
        P(),
        P("tp", None),
        P(("grp", "ep", "tp"), None),
        P(),
        P(("grp", "ep", "tp"), None),
        P(("grp", "ep", "tp"), None),
        P("ep", None, "tp"),
        P("ep", None, "tp"),
        P("ep", "tp", None),
    )
    out_specs = (P(("grp", "ep", "tp"), None), P(("grp", "ep", "tp"), None))
    return jax.shard_map(local, mesh=mesh, in_specs=in_specs, out_specs=out_specs, check_vma=False)
```

time: 144 us -> 94.3 us (0.65)
  the two profiles are of different devices: /device:TPU:8 before, /device:TPU:0 now
where the time goes in v1:
time: 94.3 us; the launch traced here: 94.1 us
  Pallas kernels  93.4 us (99%)
    pallas_call x1, Pallas kernels, fused(): pl.pallas_call(functools.partial(fused_kernel, steps, ORDER), out_shape=(...  91.5 us
    pallas_call x1, Pallas kernels, fused(): pl.pallas_call(deliver_kernel, out_shape=(jax.ShapeDtypeStruct(mixed.shap...  1.95 us

profile of v1, /device:TPU:0, one launch (start us, length us, event | category | flops | bytes accessed | tf_op | source)
XLA Modules:
  0.0 94.1 jit_solution(18378148247433860836)
XLA Ops:
  0.6 91.5 %shard_map.158 = (bf16[48,2048]{1,0:T(8,128)(2,1)}, bf16[128,2048]{1,0:T(8,128)(2,1)}) custom-call(bf16[128,2048]{1,0:T(8,128)(2,1)} %tokens_ref.1, s32[2,128]{1,0:T(2,128)} %bitcast.12, f32[2,128]{1,0:T(2,128)} %bitcast.13, f32[1,2048]{1,0:T(1,128)} %bitcast.11, bf16[2048,512]{1,0:T(8,128)(2,1)} %bitcast.8, bf16[2048,512]{1,0:T(8,128)(2,1)} %bitcast.9, ...), custom_call_target="tpu_custom_call" | custom-call | tf_op jit(solution)/shard_map/pallas_call | solution.py:690
  92.1 2.0 %shard_map.159 = (bf16[48,2048]{1,0:T(8,128)(2,1)}, bf16[128,2048]{1,0:T(8,128)(2,1)}) custom-call(bf16[48,2048]{1,0:T(8,128)(2,1)} %get-tuple-element.4.mixed_in, bf16[128,2048]{1,0:T(8,128)(2,1)} %get-tuple-element.5.expert_in), custom_call_target="tpu_custom_call" | custom-call | tf_op jit(solution)/shard_map/pallas_call | solution.py:754

commit v2 on v1

--- a/solution.py
+++ b/solution.py
@@ -221,21 +221,25 @@
 
 
 ORDER = (
-    "A10", "A11", "A31", "B31", "B11", "A30", "C31", "KV0",
-    "D31", "B00", "A20", "A21", "KV1", "B30", "C00", "C30",
-    "D30", "B10", "E31", "KV2", "D00", "B21", "C21", "E30",
-    "D21", "B20", "B01", "ATT0", "C10", "C01", "D10", "C20",
-    "ATT1", "E00", "E21", "D20", "ATT2", "ATT3", "E10", "D01",
-    "C11", "D11", "E20", "E01", "CMB0", "OUTP", "MX0", "E11",
-    "CMB2", "CMB3", "MX1", "CMB1",
+    "SEND", "BO0", "RF0", "CO0", "RF1", "DO0", "AF00", "BO1", "AF10",
+    "AF01", "AF11", "BF00", "BF10", "KV0", "CF00", "AF02", "CF10", "Y0",
+    "AF12", "Y2", "BF11", "BF01", "DF00", "BF02", "CO1", "Y1", "CF11",
+    "BF12", "DF10", "KV1", "BN0", "CF01", "DO1", "EF00", "CF12", "CF02",
+    "DF12", "EF10", "DF11", "KV2", "BN1", "GF00", "CN0", "DF01", "GF10",
+    "EF12", "DF02", "BN2", "BO2", "CN2", "EF11", "DN0", "GF12", "CN1",
+    "EO1", "EF01", "ATT0", "DN2", "ATT1", "GF11", "CO2", "EF02", "DN1",
+    "ATT2", "EN0", "GF01", "GF02", "DO2", "EO0", "EN2", "ATT3", "OUTP",
+    "EN1", "MX0", "EO2", "CMBO", "CMBN", "CMBF", "MX1",
+)
+SENDS = (
+    ("F", 0), ("X", 0), ("X", 1), ("F", 1), ("X", 2),
+    ("N", 0), ("X", 3), ("N", 1), ("F", 2), ("F", 3), ("N", 2),
 )
 VMEM_LIMIT = 58 * 1024 * 1024
-SENDS = ((1, 1), (1, 0), (3, 1), (3, 0), (2, 0), (2, 1))
 
 
 def fused_kernel(
     steps,
-    order,
     tokens_ref,
     ids_ref,
     score_ref,
@@ -263,15 +267,23 @@
     sin_ref,
     tok_ref,
     norm_ref,
-    outb,
-    rows,
+    outf,
+    scl,
+    sc,
+    orows,
+    nrows,
+    frows,
     act,
     part,
     from_core,
     to_x,
     from_x,
     total,
-    back,
+    fres,
+    comb,
+    oback,
+    nback,
+    fback,
     acc,
     lut,
     kv,
@@ -281,8 +293,12 @@
     to_xm,
     from_xm,
     hsem,
-    zs,
-    zr,
+    near_s,
+    near_r,
+    far_s,
+    far_r,
+    rel_s,
+    rel_r,
     xs,
     xr,
     cs,
@@ -291,8 +307,14 @@
     pr,
     qs,
     qr,
-    bs,
-    br,
+    nb_s,
+    nb_r,
+    fo_s,
+    fo_r,
+    fb_s,
+    fb_r,
+    sc_s,
+    sc_r,
     ks,
     kr,
     ms,
@@ -302,8 +324,12 @@
     lane = lax.axis_index("tp")
     peers = [flip(me, k) for k in range(steps)]
     core, across = flip(lane, 1), flip(lane, 2)
-    cap, width = outb.shape[1], outb.shape[2]
-    half = cap // 2
+    inner = ((me + 1) // 2) % 2
+    outer = 1 - inner
+    gate_at = 2 - me // 2
+    sources = [3 - me, flip(3 - me, 1)]
+    blocks, _, size, width = orows.shape
+    wide = blocks - 1
     hidden = gate_ref.shape[1]
     length = query_ref.shape[0]
     dim = keyraw_ref.shape[1]
@@ -349,32 +375,122 @@
             device_id_type=MESH,
         )
 
-    def piece(h):
-        return pl.ds(h * half, half)
-
-    units = [(k, h) for k in range(steps) for h in range(2)]
-    z_in, x_in, c_in, c_out, x_out, z_out = {}, {}, {}, {}, {}, {}
-    for k, h in units:
-        n = 2 * k + h
-        if k:
-            z_in[k, h] = remote(
-                outb.at[k, piece(h)], rows.at[k, h, 0], zs.at[n], zr.at[n], peers[k], lane
+    def when_inner(body):
+        pl.when(inner == 1)(body)
+
+    def when_outer(body):
+        pl.when(inner == 0)(body)
+
+    kinds = ("O", "N", "F0", "F1")
+    window = range(wide)
+    number = {(c, i): n * wide + i for n, c in enumerate(kinds) for i in window}
+
+    def rows_of(c, i):
+        if c == "O":
+            return orows.at[i + inner]
+        if c == "N":
+            return nrows.at[i]
+        return frows.at[int(c[1]), i + inner]
+
+    def x_own(p):
+        return remote(orows.at[p, 0], orows.at[p, 1], xs.at[p], xr.at[p], me, across)
+
+    near = [
+        [
+            remote(
+                orows.at[i + outer, n],
+                nrows.at[i, n],
+                near_s.at[n * wide + i],
+                near_r.at[n * wide + i],
+                peers[1],
+                lane,
             )
-            z_out[k, h] = remote(
-                total.at[k, h], back.at[k, piece(h)], bs.at[n], br.at[n], peers[k], lane
+            for i in window
+        ]
+        for n in range(2)
+    ]
+    far = [
+        remote(
+            outf.at[p],
+            frows.at[outer, p, 0],
+            far_s.at[p],
+            far_r.at[outer * blocks + p],
+            gate_at,
+            lane,
+        )
+        for p in range(blocks)
+    ]
+    far_in = [
+        [
+            remote(
+                outf.at[p], frows.at[j, p, 0], far_s.at[p], far_r.at[j * blocks + p], gate_at, lane
             )
-        x_in[k, h] = remote(rows.at[k, h, 0], rows.at[k, h, 1], xs.at[n], xr.at[n], me, across)
-        c_in[k, h] = remote(
-            rows.at[k, h, pl.ds(0, 2)], rows.at[k, h, pl.ds(2, 2)], cs.at[n], cr.at[n], me, core
-        )
-        c_out[k, h] = remote(
-            part.at[k, h, pl.ds(2, 2)], from_core.at[k, h], ps.at[n], pr.at[n], me, core
-        )
-        x_out[k, h] = remote(to_x.at[k, h], from_x.at[k, h], qs.at[n], qr.at[n], me, across)
+            for p in range(blocks)
+        ]
+        for j in range(2)
+    ]
+    relay = [
+        [
+            remote(
+                frows.at[j, p, 0],
+                frows.at[j, p, 0],
+                rel_s.at[j * wide + p],
+                rel_r.at[j * wide + p],
+                peers[1],
+                lane,
+            )
+            for p in window
+        ]
+        for j in range(2)
+    ]
+    scale_out = remote(scl, sc.at[outer], sc_s.at[0], sc_r.at[outer], gate_at, lane)
+    scale_in = [remote(scl, sc.at[j], sc_s.at[0], sc_r.at[j], gate_at, lane) for j in range(2)]
+    x_far, c_in, c_out, x_out = {}, {}, {}, {}
+    for (c, i), u in number.items():
+        held = rows_of(c, i)
+        if c[0] == "F":
+            at = blocks + u - 2 * wide
+            x_far[c, i] = remote(held.at[0], held.at[1], xs.at[at], xr.at[at], me, across)
+        c_in[c, i] = remote(
+            held.at[pl.ds(0, 2)], held.at[pl.ds(2, 2)], cs.at[u], cr.at[u], me, core
+        )
+        c_out[c, i] = remote(
+            part.at[u, pl.ds(2, 2)], from_core.at[u], ps.at[u], pr.at[u], me, core
+        )
+        x_out[c, i] = remote(to_x.at[u], from_x.at[u], qs.at[u], qr.at[u], me, across)
+    near_back = [
+        remote(total.at[wide + i], nback.at[i], nb_s.at[i], nb_r.at[i], peers[1], lane)
+        for i in window
+    ]
+    far_over = [
+        [
+            remote(
+                total.at[(2 + j) * wide + i],
+                fres.at[j, i],
+                fo_s.at[j * wide + i],
+                fo_r.at[j * wide + i],
+                peers[1],
+                lane,
+            )
+            for i in window
+        ]
+        for j in range(2)
+    ]
+
+    def far_back(j, p):
+        if p == 0:
+            source = fres.at[j, 0]
+        elif p == wide:
+            source = total.at[(2 + j) * wide + wide - 1]
+        else:
+            source = comb.at[j, p - 1]
+        return remote(
+            source, fback.at[p], fb_s.at[j * blocks + p], fb_r.at[p], sources[j], lane
+        )
+
     kv_near = remote(kv.at[0], kv.at[1], ks.at[0], kr.at[0], peers[1], lane)
     kv_mid = remote(kv.at[pl.ds(0, 2)], kv.at[pl.ds(2, 2)], ks.at[1], kr.at[1], peers[3], lane)
     kv_far = remote(kv.at[pl.ds(2, 2)], kv.at[pl.ds(2, 2)], ks.at[2], kr.at[2], peers[1], lane)
-    inner = (me == 1) | (me == 2)
     m_core = [
         remote(pm.at[core], fc.at[0], ms.at[0], mr.at[0], me, core),
         remote(pm.at[flip(core, 2)], fc.at[1], ms.at[1], mr.at[1], me, core),
@@ -387,50 +503,120 @@
     first, second = ids_ref[0:1, :], ids_ref[1:2, :]
     weight = 1.0 / (1.0 + jnp.exp(score_ref[1:2, :] - score_ref[0:1, :]))
     table_row = lax.broadcasted_iota(jnp.int32, (8, count), 0)
-    named = jnp.zeros((8, count), f32)
-    scale = jnp.zeros((8, count), f32)
-    for k in range(steps):
-        one, two = first == peers[k], second == peers[k]
-        here = jnp.where(one | two, 1.0, 0.0)
-        named = jnp.where(table_row == k, here, named)
-        value = jnp.where(one, weight, 0.0) + jnp.where(two, 1.0 - weight, 0.0)
-        scale = jnp.where(table_row == k, value, scale)
-    rank = jnp.dot(named.astype(b16), earlier, preferred_element_type=f32)
-    place = jnp.where(named > 0.5, rank, -1.0)
-    rest = jnp.zeros((count - 16, count), f32)
-    lut[...] = jnp.transpose(jnp.concatenate([place, scale, rest], axis=0))
+    high = me // 2
+    ends = (3 * high, 3 - 3 * high)
+    middles = (1 + high, 2 - high)
+
+    def naming(expert):
+        one, two = first == expert, second == expert
+        share = jnp.where(one, weight, 0.0) + jnp.where(two, 1.0 - weight, 0.0)
+        return jnp.where(one | two, 1.0, 0.0), share
+
+    named = [(naming(ends[n]), naming(middles[n])) for n in range(2)]
+    counted = jnp.zeros((8, count), f32)
+    parts_of = []
+    for n in range(2):
+        (end_one, _), (mid_one, _) = named[n]
+        both = end_one * mid_one
+        parts_of.append((end_one - both, mid_one - both, both))
+        for r in range(3):
+            counted = jnp.where(table_row == 3 * n + r, parts_of[n][r], counted)
+    rank = jnp.dot(counted.astype(b16), earlier, preferred_element_type=f32)
+    sums = jnp.sum(counted, axis=1, keepdims=True)
+    tail, middle = float(size), float(size * (wide - 1))
+
+    def positions(n):
+        end_only, mid_only, both = parts_of[n]
+        end_rank, mid_rank, both_rank = (rank[3 * n + r : 3 * n + r + 1, :] for r in range(3))
+        end_sum, both_sum = sums[3 * n : 3 * n + 1, :], sums[3 * n + 2 : 3 * n + 3, :]
+        extra = jnp.maximum(both_sum - middle, 0.0)
+        common = tail + jnp.minimum(both_sum, middle)
+        end_at, mid_at = end_rank + extra, mid_rank + extra
+        spill = jnp.maximum(end_sum + extra - tail, 0.0)
+        shared = both_rank < middle
+        end_pos = jnp.where(
+            both > 0.5,
+            jnp.where(shared, tail + both_rank, both_rank - middle),
+            jnp.where(end_at < tail, end_at, common + end_at - tail),
+        )
+        mid_pos = jnp.where(
+            both > 0.5,
+            tail + both_rank,
+            jnp.where(
+                mid_at < tail, tail + middle + mid_at, common + spill + mid_at - tail
+            ),
+        )
+        end_pos = jnp.where(end_only + both > 0.5, end_pos, -1.0)
+        mid_pos = jnp.where(mid_only + both > 0.5, mid_pos, -1.0)
+        return end_pos, mid_pos, jnp.where((both > 0.5) & shared, 1.0, 0.0)
+
+    own_end, own_mid, _ = positions(0)
+    far_end, far_mid, far_shared = positions(1)
+    slot = lax.broadcasted_iota(jnp.int32, (count, count), 0).astype(f32)
+
+    def dispatch(end_pos, mid_pos):
+        chosen = ((slot == end_pos) | (slot == mid_pos)).astype(b16)
+        picked = jnp.dot(chosen, norm_ref[...], preferred_element_type=f32)
+        return picked.astype(b16).reshape(blocks, size, width)
 
     loads[0].wait()
-    values = tok_ref[...].astype(f32)
-    norm_ref[...] = (
-        values
-        * lax.rsqrt(jnp.mean(values * values, axis=-1, keepdims=True) + EPS)
-        * ngain_ref[...]
-    ).astype(b16)
-
-    slot = lax.broadcasted_iota(jnp.int32, (cap, count), 0).astype(f32)
-
-    def dispatch(k):
-        chosen = (slot == place[k : k + 1, :]).astype(b16)
-        picked = jnp.dot(chosen, norm_ref[...], preferred_element_type=f32).astype(b16)
-        if k:
-            outb[k] = picked
-        else:
-            rows[0, 0, 0] = picked[:half]
-            rows[0, 1, 0] = picked[half:]
-
-    sent = {SENDS[0][0], 0}
-    dispatch(SENDS[0][0])
-    dispatch(0)
+    for n in range(blocks):
+        spot = pl.ds(n * size, size)
+        values = tok_ref[spot, :].astype(f32)
+        norm_ref[spot, :] = (
+            values
+            * lax.rsqrt(jnp.mean(values * values, axis=-1, keepdims=True) + EPS)
+            * ngain_ref[...]
+        ).astype(b16)
+    outf[...] = dispatch(far_end, far_mid)
     pl.semaphore_wait(barrier, len(friends))
-    z_in[SENDS[0]].start()
-    for h in range(2):
-        x_in[0, h].start()
-    for k, h in SENDS[1:]:
-        if k not in sent:
-            sent.add(k)
-            dispatch(k)
-        z_in[k, h].start()
+    far[0].start()
+    orows[:, 0] = dispatch(own_end, own_mid)
+
+    def stage_send():
+        for kind, p in SENDS:
+            if kind == "F" and p > 0:
+                far[p].start()
+            elif kind == "X":
+                x_own(p).start()
+            elif kind == "N":
+                near[0][p].start()
+        end_share, mid_share = named[1][0][1], named[1][1][1]
+        rows_mid = slice(size, size * wide)
+        end_scale = jnp.sum(
+            jnp.where(
+                slot[rows_mid] == far_end, jnp.where(far_shared > 0.5, end_share, 1.0), 0.0
+            ),
+            axis=1,
+            keepdims=True,
+        )
+        mid_scale = jnp.sum(
+            jnp.where(
+                slot[rows_mid] == far_mid, jnp.where(far_shared > 0.5, mid_share, 1.0), 0.0
+            ),
+            axis=1,
+            keepdims=True,
+        )
+        lanes_of = lax.broadcasted_iota(jnp.int32, scl.shape, 1)
+        scl[...] = jnp.where(lanes_of < scl.shape[1] // 2, end_scale, mid_scale)
+        scale_out.start()
+        is_inner = (jnp.zeros((1, count), jnp.int32) + inner) == 1
+        own_mid_at = jnp.where(own_mid < 0.0, -1.0, own_mid - tail)
+        table = (
+            jnp.where(is_inner, own_mid_at, own_end),
+            jnp.where(is_inner, own_end, own_mid_at),
+            far_end,
+            jnp.where(far_shared > 0.5, -1.0, far_mid),
+            jnp.where(is_inner, named[0][1][1], named[0][0][1]),
+            jnp.where(is_inner, named[0][0][1], named[0][1][1]),
+            jnp.where(far_shared > 0.5, 1.0, end_share),
+            mid_share,
+        )
+        kept = jnp.zeros((8, count), f32)
+        for r in range(8):
+            kept = jnp.where(table_row == r, table[r], kept)
+        rest = jnp.zeros((count - 8, count), f32)
+        lut[...] = jnp.transpose(jnp.concatenate([kept, rest], axis=0))
 
     turn_lane = lax.broadcasted_iota(jnp.int32, (length, dim), 1)
     leading = (turn_lane // (dim // 4)) % 2 == 0
@@ -449,78 +635,137 @@
         )
         return (vectors * cos_ref[...] + other * sin_ref[...]).astype(b16)
 
-    def stage_a(k, h):
-        z_in[k, h].wait_recv()
-        x_in[k, h].start()
-
-    def stage_b(k, h):
-        x_in[k, h].wait_recv()
-        c_in[k, h].start()
-
-    def stage_c(k, h):
-        c_in[k, h].wait_recv()
+    arrived = (set(), set())
+
+    def own_arrived(by_role):
+        missing = [p not in arrived[r] for r, p in enumerate(by_role)]
+        for r, p in enumerate(by_role):
+            arrived[r].add(p)
+        for r, run in ((0, when_outer), (1, when_inner)):
+            if missing[r]:
+
+                @run
+                def _(p=by_role[r]):
+                    x_own(p).wait_recv()
+
+    def stage_y(i):
+        own_arrived((i + 1, i))
+        near[1][i].start()
+
+    def stage_a(c, i):
+        j = int(c[1])
+
+        @when_inner
+        def _():
+            far_in[j][i + 1].wait_recv()
+            if i + 1 < wide:
+                relay[j][i + 1].start()
+
+        @when_outer
+        def _():
+            relay[j][i].wait_recv()
+
+        x_far[c, i].start()
+
+    def stage_r(j):
+        @when_inner
+        def _():
+            far_in[j][0].wait_recv()
+            relay[j][0].start()
+
+    def stage_b(c, i):
+        if c == "O":
+            own_arrived((i, i + 1))
+        elif c == "N":
+            near[0][i].wait_recv()
+            near[1][i].wait_recv()
+        else:
+            x_far[c, i].wait_recv()
+        c_in[c, i].start()
+
+    def stage_c(c, i):
+        c_in[c, i].wait_recv()
+        u = number[c, i]
+        held = rows_of(c, i)
 
         @pl.loop(0, hidden // tile)
-        def _(i):
-            cols = pl.ds(pl.multiple_of(i * tile, tile), tile)
-            block = rows[k, h].reshape(4 * half, width)
+        def _(n):
+            cols = pl.ds(pl.multiple_of(n * tile, tile), tile)
+            block = held[...].reshape(4 * size, width)
             gate = jnp.dot(block, gate_ref[:, cols], preferred_element_type=f32)
             up = jnp.dot(block, up_ref[:, cols], preferred_element_type=f32)
             act[:, cols] = (gate / (1.0 + jnp.exp(-gate)) * up).astype(b16)
 
         @pl.loop(0, width // tile_out)
-        def _(i):
-            cols = pl.ds(pl.multiple_of(i * tile_out, tile_out), tile_out)
+        def _(n):
+            cols = pl.ds(pl.multiple_of(n * tile_out, tile_out), tile_out)
             summed = jnp.dot(act[...], down_ref[:, cols], preferred_element_type=f32)
-            part[k, h, :, :, cols] = summed.astype(b16).reshape(4, half, tile_out)
-
-        c_out[k, h].start()
-
-    def stage_d(k, h):
-        c_out[k, h].wait_recv()
-        to_x[k, h] = (part[k, h, 1].astype(f32) + from_core[k, h, 1].astype(f32)).astype(b16)
-        x_out[k, h].start()
-
-    def stage_e(k, h):
-        x_out[k, h].wait_recv()
+            part[u, :, :, cols] = summed.astype(b16).reshape(4, size, tile_out)
+
+        c_out[c, i].start()
+
+    def stage_d(c, i):
+        c_out[c, i].wait_recv()
+        u = number[c, i]
+        to_x[u] = (part[u, 1].astype(f32) + from_core[u, 1].astype(f32)).astype(b16)
+        x_out[c, i].start()
+
+    def stage_e(c, i):
+        x_out[c, i].wait_recv()
+        u = number[c, i]
         summed = (
-            part[k, h, 0].astype(f32) + from_core[k, h, 0].astype(f32) + from_x[k, h].astype(f32)
+            part[u, 0].astype(f32) + from_core[u, 0].astype(f32) + from_x[u].astype(f32)
         ).astype(b16)
-        if k == 0:
-            back[0, piece(h)] = summed
+        if c == "O":
+            oback[i] = summed
+            return
+        total[u] = summed
+        if c == "N":
+            near_back[i].start()
+            return
+        j = int(c[1])
+        when_outer(far_over[j][i].start)
+        if i == wide - 1:
+            when_inner(far_back(j, wide).start)
+
+    def stage_g(j, p):
+        if p > 0 and j not in scaled:
+            scaled.add(j)
+            when_inner(scale_in[j].wait_recv)
+
+        @when_inner
+        def _():
+            far_over[j][p].wait_recv()
+            if p > 0:
+                spot = pl.ds((p - 1) * size, size)
+                end_scale = sc[j, spot, 0:1]
+                mid_scale = sc[j, spot, sc.shape[2] // 2 : sc.shape[2] // 2 + 1]
+                comb[j, p - 1] = (
+                    end_scale * fres[j, p].astype(f32)
+                    + mid_scale * total[(2 + j) * wide + p - 1].astype(f32)
+                ).astype(b16)
+            far_back(j, p).start()
+
+    def stage_kv(step):
+        if step == 0:
+            for n in range(1, 5):
+                loads[n].wait()
+            kv[0, 0] = turned(keyraw_ref[...], kgain_ref)
+            kv_near.start()
+        elif step == 1:
+            kv_near.wait_recv()
+            when_inner(kv_mid.start)
         else:
-            total[k, h] = summed
-            z_out[k, h].start()
-
-    def stage_kv0():
-        loads[1].wait()
-        loads[2].wait()
-        loads[3].wait()
-        loads[4].wait()
-        kv[0, 0] = turned(keyraw_ref[...], kgain_ref)
-        kv_near.start()
-
-    def stage_kv1():
-        kv_near.wait_recv()
-
-        @pl.when(inner)
-        def _():
-            kv_mid.start()
-
-    def stage_kv2():
-        @pl.when(inner)
-        def _():
-            kv_mid.wait_recv()
-            kv_far.start()
+
+            @when_inner
+            def _():
+                kv_mid.wait_recv()
+                kv_far.start()
 
     def stage_att(head):
         if head == 0:
             loads[5].wait()
-
-            @pl.when(jnp.logical_not(inner))
-            def _():
-                kv_far.wait_recv()
-
+            when_outer(kv_far.wait_recv)
         cols = slice(head * dim, (head + 1) * dim)
         held = steps * length
         queries = turned(query_ref[:, cols], qgain_ref)
@@ -563,21 +808,33 @@
             ).astype(b16)
 
     combined = []
-
-    def stage_cmb(k):
-        if k > 0:
-            for h in range(2):
-                z_out[k, h].wait_recv()
-        spot = lax.broadcasted_iota(jnp.int32, (count, cap), 1).astype(f32)
-        chosen = (spot == lut[:, k : k + 1]).astype(b16)
-        scaled = lut[:, 8 + k : 9 + k]
-        opening, closing = not combined, len(combined) == steps - 1
-        combined.append(k)
+    scaled = set()
+
+    def stage_cmb(c):
+        opening, closing = not combined, len(combined) == 2
+        combined.append(c)
+        if c == "N":
+            for i in window:
+                near_back[i].wait_recv()
+        if c == "F":
+            for p in range(blocks):
+                far_back(0, p).wait_recv()
+        store = {"O": oback, "N": nback, "F": fback}[c]
+        columns = {"O": (0,), "N": (1,), "F": (2, 3)}[c]
+        depth = store.shape[0] * size
+        spot = lax.broadcasted_iota(jnp.int32, (count, depth), 1).astype(f32)
+        chosen = jnp.concatenate(
+            [(spot == lut[:, r : r + 1]).astype(b16) for r in columns], axis=0
+        )
 
         @pl.loop(0, width // tile_out)
         def _(i):
             cols = pl.ds(pl.multiple_of(i * tile_out, tile_out), tile_out)
-            found = scaled * jnp.dot(chosen, back[k, :, cols], preferred_element_type=f32)
+            results = store[:, :, cols].reshape(depth, tile_out)
+            picked = jnp.dot(chosen, results, preferred_element_type=f32)
+            found = lut[:, 4 + columns[0] : 5 + columns[0]] * picked[:count]
+            if c == "F":
+                found = found + lut[:, 7:8] * picked[count:]
             if not opening:
                 found = acc[:, cols] + found
             if closing:
@@ -587,34 +844,60 @@
 
     stages = {"A": stage_a, "B": stage_b, "C": stage_c, "D": stage_d, "E": stage_e}
     loaded = False
-    for name in order:
-        if name[0] == "C" and name[1] != "M" and not loaded:
-            loaded = True
-            for n in (6, 7, 8):
-                loads[n].wait()
-        if name.startswith("KV"):
-            (stage_kv0, stage_kv1, stage_kv2)[int(name[2])]()
-        elif name.startswith("ATT"):
+    for name in ORDER:
+        if name == "SEND":
+            stage_send()
+        elif name[:2] == "KV":
+            stage_kv(int(name[2]))
+        elif name[:3] == "ATT":
             stage_att(int(name[3]))
         elif name == "OUTP":
             stage_outp()
-        elif name.startswith("MX"):
+        elif name[:2] == "MX":
             stage_mx(int(name[2]))
-        elif name.startswith("CMB"):
-            stage_cmb(int(name[3]))
+        elif name[:3] == "CMB":
+            stage_cmb(name[3])
+        elif name[0] == "Y":
+            stage_y(int(name[1]))
+        elif name[0] == "R":
+            stage_r(int(name[2]))
+        elif name[0] == "G":
+            stage_g(int(name[2]), int(name[3]))
         else:
-            stages[name[0]](int(name[1]), int(name[2]))
-
-    for unit in units:
-        for table in (z_in, x_in, c_in, c_out, x_out, z_out):
-            if unit in table:
-                table[unit].wait_send()
+            if name[0] == "C" and not loaded:
+                loaded = True
+                for n in (6, 7, 8):
+                    loads[n].wait()
+            stages[name[0]](name[1:-1], int(name[-1]))
+
+    for p in range(blocks):
+        x_own(p).wait_send()
+        far[p].wait_send()
+    for table in (x_far, c_in, c_out, x_out):
+        for copy in table.values():
+            copy.wait_send()
+    for i in window:
+        near[0][i].wait_send()
+        near[1][i].wait_send()
+        near_back[i].wait_send()
+    scale_out.wait_send()
     kv_near.wait_send()
 
-    @pl.when(inner)
+    @when_inner
     def _():
         kv_mid.wait_send()
         kv_far.wait_send()
+        for j in range(2):
+            for i in window:
+                relay[j][i].wait_send()
+            for p in range(blocks):
+                far_back(j, p).wait_send()
+
+    @when_outer
+    def _():
+        for j in range(2):
+            for i in window:
+                far_over[j][i].wait_send()
 
     for copy in m_core:
         copy.wait_send()
@@ -679,16 +962,18 @@
     steps, lanes = lax.axis_size("ep"), lax.axis_size("tp")
     count, width = mix_tokens.shape
     cap = count * expert_ids.shape[1] * 3 // (2 * steps)
-    half = cap // 2
+    size = count - cap
+    blocks = count // size
+    wide = blocks - 1
     hidden = gate_proj.shape[2]
     length, dim = projected_keys.shape
     kind = jnp.bfloat16
     cosine, sine = turn_tables(steps * length, dim)
     vmem = pl.BlockSpec(memory_space=pltpu.VMEM)
     anywhere = pl.BlockSpec(memory_space=pltpu.HBM)
-    units = 2 * steps
+    units = 4 * wide
     mixed, expert = pl.pallas_call(
-        functools.partial(fused_kernel, steps, ORDER),
+        functools.partial(fused_kernel, steps),
         out_shape=(
             jax.ShapeDtypeStruct((length // lanes, width), kind),
             jax.ShapeDtypeStruct((count, width), kind),
@@ -710,15 +995,23 @@
             pltpu.VMEM((length, dim), jnp.float32),
             pltpu.VMEM((count, width), kind),
             pltpu.VMEM((count, width), kind),
-            pltpu.VMEM((steps, cap, width), kind),
-            pltpu.VMEM((steps, 2, 4, half, width), kind),
-            pltpu.VMEM((4 * half, hidden), kind),
-            pltpu.VMEM((steps, 2, 4, half, width), kind),
-            pltpu.VMEM((steps, 2, 2, half, width), kind),
-            pltpu.VMEM((steps, 2, half, width), kind),
-            pltpu.VMEM((steps, 2, half, width), kind),
-            pltpu.VMEM((steps, 2, half, width), kind),
-            pltpu.VMEM((steps, cap, width), kind),
+            pltpu.VMEM((blocks, size, width), kind),
+            pltpu.VMEM((size * (wide - 1), 128), jnp.float32),
+            pltpu.VMEM((2, size * (wide - 1), 128), jnp.float32),
+            pltpu.VMEM((blocks, 4, size, width), kind),
+            pltpu.VMEM((wide, 4, size, width), kind),
+            pltpu.VMEM((2, blocks, 4, size, width), kind),
+            pltpu.VMEM((4 * size, hidden), kind),
+            pltpu.VMEM((units, 4, size, width), kind),
+            pltpu.VMEM((units, 2, size, width), kind),
+            pltpu.VMEM((units, size, width), kind),
+            pltpu.VMEM((units, size, width), kind),
+            pltpu.VMEM((units, size, width), kind),
+            pltpu.VMEM((2, wide, size, width), kind),
+            pltpu.VMEM((2, wide - 1, size, width), kind),
+            pltpu.VMEM((wide, size, width), kind),
+            pltpu.VMEM((wide, size, width), kind),
+            pltpu.VMEM((blocks, size, width), kind),
             pltpu.VMEM((count, width), jnp.float32),
             pltpu.VMEM((count, count), jnp.float32),
             pltpu.VMEM((steps, 2, length, dim), kind),
@@ -729,8 +1022,11 @@
             pltpu.VMEM((length // lanes, width), kind),
             pltpu.SemaphoreType.DMA((10,)),
         ]
-        + [pltpu.SemaphoreType.DMA((units,))] * 12
-        + [pltpu.SemaphoreType.DMA((3,))] * 4,
+        + [pltpu.SemaphoreType.DMA((2 * blocks,))] * 6
+        + [pltpu.SemaphoreType.DMA((blocks + 2 * wide,))] * 2
+        + [pltpu.SemaphoreType.DMA((units,))] * 6
+        + [pltpu.SemaphoreType.DMA((2 * blocks,))] * 6
+        + [pltpu.SemaphoreType.DMA((3,))] * 6,
         compiler_params=pltpu.CompilerParams(
             collective_id=0, has_side_effects=True, vmem_limit_bytes=VMEM_LIMIT
         ),
@@ -784,7 +1080,10 @@
         and length % 64 == 0
         and length <= 256
         and count == 128
-        and cap % 32 == 0
+        and cap < count
+        and (count - cap) % 16 == 0
+        and cap % (count - cap) == 0
+        and 2 * cap > count
         and blocks < 48 * 1024 * 1024
     )
 

time: 94.3 us -> 83.2 us (0.88)
  Pallas kernels: 93.4 us -> 82.4 us
    pallas_call x1, Pallas kernels: 91.5 us -> 80.5 us  [fused(): pl.pallas_call(functools.partial(fused_kernel, steps), out_shape=(jax.Sha...]
where the time goes in v2:
time: 83.2 us; the launch traced here: 83 us
  Pallas kernels  82.4 us (99%)
    pallas_call x1, Pallas kernels, fused(): pl.pallas_call(functools.partial(fused_kernel, steps), out_shape=(jax.Sha...  80.5 us
    pallas_call x1, Pallas kernels, fused(): pl.pallas_call(deliver_kernel, out_shape=(jax.ShapeDtypeStruct(mixed.shap...  1.95 us

profile of v2, /device:TPU:0, one launch (start us, length us, event | category | flops | bytes accessed | tf_op | source)
XLA Modules:
  0.0 83.0 jit_solution(3679685983309359700)
XLA Ops:
  0.6 80.5 %shard_map.158 = (bf16[48,2048]{1,0:T(8,128)(2,1)}, bf16[128,2048]{1,0:T(8,128)(2,1)}) custom-call(bf16[128,2048]{1,0:T(8,128)(2,1)} %tokens_ref.1, s32[2,128]{1,0:T(2,128)} %bitcast.12, f32[2,128]{1,0:T(2,128)} %bitcast.13, f32[1,2048]{1,0:T(1,128)} %bitcast.11, bf16[2048,512]{1,0:T(8,128)(2,1)} %bitcast.8, bf16[2048,512]{1,0:T(8,128)(2,1)} %bitcast.9, ...), custom_call_target="tpu_custom_call" | custom-call | tf_op jit(solution)/shard_map/pallas_call | solution.py:975
  81.1 2.0 %shard_map.159 = (bf16[48,2048]{1,0:T(8,128)(2,1)}, bf16[128,2048]{1,0:T(8,128)(2,1)}) custom-call(bf16[48,2048]{1,0:T(8,128)(2,1)} %get-tuple-element.4.mixed_in, bf16[128,2048]{1,0:T(8,128)(2,1)} %get-tuple-element.5.expert_in), custom_call_target="tpu_custom_call" | custom-call | tf_op jit(solution)/shard_map/pallas_call | solution.py:1050

commit v3 on v2

--- a/solution.py
+++ b/solution.py
@@ -221,29 +221,29 @@
 
 
 ORDER = (
-    "SEND", "BO0", "RF0", "CO0", "RF1", "DO0", "AF00", "BO1", "AF10",
-    "AF01", "AF11", "BF00", "BF10", "KV0", "CF00", "AF02", "CF10", "Y0",
-    "AF12", "Y2", "BF11", "BF01", "DF00", "BF02", "CO1", "Y1", "CF11",
-    "BF12", "DF10", "KV1", "BN0", "CF01", "DO1", "EF00", "CF12", "CF02",
-    "DF12", "EF10", "DF11", "KV2", "BN1", "GF00", "CN0", "DF01", "GF10",
-    "EF12", "DF02", "BN2", "BO2", "CN2", "EF11", "DN0", "GF12", "CN1",
-    "EO1", "EF01", "ATT0", "DN2", "ATT1", "GF11", "CO2", "EF02", "DN1",
-    "ATT2", "EN0", "GF01", "GF02", "DO2", "EO0", "EN2", "ATT3", "OUTP",
-    "EN1", "MX0", "EO2", "CMBO", "CMBN", "CMBF", "MX1",
+    "SEND", "PRE", "BO2", "RF1", "CO2", "DO2", "AF10", "BO1", "RF0",
+    "AF11", "CO1", "AF00", "AF12", "BF11", "KV0", "AF01", "BF10", "Y1",
+    "Y0", "CF11", "CF10", "DF11", "KV1", "DF10", "BF12", "BF01", "BF00",
+    "Y2", "EO2", "CF12", "AF02", "EF11", "DF12", "KV2", "CF01", "BN0",
+    "CF00", "DF00", "DF01", "BF02", "DO1", "EF10", "EF12", "CF02", "BN1",
+    "CN0", "BN2", "ATT0", "GF10", "GF11", "EF00", "ATT1", "DF02", "GF12",
+    "BO0", "CN1", "DN0", "EF01", "GF00", "CN2", "DN1", "CO0", "EF02",
+    "ATT2", "EO1", "DN2", "ATT3", "DO0", "EN0", "EN1", "OUTP", "GF02",
+    "GF01", "EN2", "MX0", "EO0", "CMB", "MX1",
 )
 SENDS = (
-    ("F", 0), ("X", 0), ("X", 1), ("F", 1), ("X", 2),
-    ("N", 0), ("X", 3), ("N", 1), ("F", 2), ("F", 3), ("N", 2),
+    ("F", 0), ("F", 1), ("N", 0), ("F", 2), ("N", 1),
+    ("X", 3), ("N", 2), ("F", 3), ("X", 2), ("X", 1), ("X", 0),
 )
 VMEM_LIMIT = 58 * 1024 * 1024
 
 
 def fused_kernel(
     steps,
-    tokens_ref,
-    ids_ref,
-    score_ref,
-    ngain_ref,
+    tokens_hbm,
+    ids_hbm,
+    score_hbm,
+    ngain_hbm,
     gate_hbm,
     up_hbm,
     down_hbm,
@@ -251,12 +251,20 @@
     query_hbm,
     key_hbm,
     value_hbm,
+    qgain_hbm,
+    kgain_hbm,
+    cos_hbm,
+    sin_hbm,
+    mixed_hbm,
+    expert_hbm,
+    ids_ref,
+    score_ref,
+    ngain_ref,
     qgain_ref,
     kgain_ref,
-    cos_hbm,
-    sin_hbm,
     mixed_ref,
     expert_ref,
+    pick,
     gate_ref,
     up_ref,
     down_ref,
@@ -284,7 +292,6 @@
     oback,
     nback,
     fback,
-    acc,
     lut,
     kv,
     heads_ref,
@@ -293,6 +300,7 @@
     to_xm,
     from_xm,
     hsem,
+    osem,
     near_s,
     near_r,
     far_s,
@@ -343,11 +351,16 @@
         pltpu.make_async_copy(s, d, hsem.at[i])
         for i, (s, d) in enumerate(
             [
-                (tokens_ref, tok_ref),
+                (ids_hbm, ids_ref),
+                (score_hbm, score_ref),
+                (tokens_hbm, tok_ref),
+                (ngain_hbm, ngain_ref),
+                (kgain_hbm, kgain_ref),
                 (key_hbm, keyraw_ref),
                 (value_hbm, kv.at[0, 1]),
                 (cos_hbm.at[pl.ds(offset, length)], cos_ref),
                 (sin_hbm.at[pl.ds(offset, length)], sin_ref),
+                (qgain_hbm, qgain_ref),
                 (query_hbm, query_ref),
                 (gate_hbm, gate_ref),
                 (up_hbm, up_ref),
@@ -496,6 +509,18 @@
         remote(pm.at[flip(core, 2)], fc.at[1], ms.at[1], mr.at[1], me, core),
     ]
     m_x = remote(to_xm, from_xm, ms.at[2], mr.at[2], me, across)
+    mixed_out = pltpu.make_async_copy(mixed_ref, mixed_hbm, osem.at[0])
+    expert_out = [
+        pltpu.make_async_copy(
+            expert_ref.at[:, pl.ds(n * tile_out, tile_out)],
+            expert_hbm.at[:, pl.ds(n * tile_out, tile_out)],
+            osem.at[1 + n],
+        )
+        for n in range(width // tile_out)
+    ]
+
+    loads[0].wait()
+    loads[1].wait()
 
     token_row = lax.broadcasted_iota(jnp.int32, (count, count), 0)
     token_col = lax.broadcasted_iota(jnp.int32, (count, count), 1)
@@ -559,7 +584,8 @@
         picked = jnp.dot(chosen, norm_ref[...], preferred_element_type=f32)
         return picked.astype(b16).reshape(blocks, size, width)
 
-    loads[0].wait()
+    loads[2].wait()
+    loads[3].wait()
     for n in range(blocks):
         spot = pl.ds(n * size, size)
         values = tok_ref[spot, :].astype(f32)
@@ -636,6 +662,7 @@
         return (vectors * cos_ref[...] + other * sin_ref[...]).astype(b16)
 
     arrived = (set(), set())
+    scaled = set()
 
     def own_arrived(by_role):
         missing = [p not in arrived[r] for r, p in enumerate(by_role)]
@@ -748,7 +775,7 @@
 
     def stage_kv(step):
         if step == 0:
-            for n in range(1, 5):
+            for n in range(4, 9):
                 loads[n].wait()
             kv[0, 0] = turned(keyraw_ref[...], kgain_ref)
             kv_near.start()
@@ -764,7 +791,8 @@
 
     def stage_att(head):
         if head == 0:
-            loads[5].wait()
+            loads[9].wait()
+            loads[10].wait()
             when_outer(kv_far.wait_recv)
         cols = slice(head * dim, (head + 1) * dim)
         held = steps * length
@@ -784,7 +812,7 @@
         heads_ref[:, cols] = (summed / amount).astype(b16)
 
     def stage_outp():
-        loads[9].wait()
+        loads[14].wait()
 
         @pl.loop(0, width // tile_out)
         def _(i):
@@ -806,41 +834,30 @@
             mixed_ref[...] = (
                 pm[lane].astype(f32) + fc[0].astype(f32) + from_xm[...].astype(f32)
             ).astype(b16)
-
-    combined = []
-    scaled = set()
-
-    def stage_cmb(c):
-        opening, closing = not combined, len(combined) == 2
-        combined.append(c)
-        if c == "N":
-            for i in window:
-                near_back[i].wait_recv()
-        if c == "F":
-            for p in range(blocks):
-                far_back(0, p).wait_recv()
-        store = {"O": oback, "N": nback, "F": fback}[c]
-        columns = {"O": (0,), "N": (1,), "F": (2, 3)}[c]
-        depth = store.shape[0] * size
-        spot = lax.broadcasted_iota(jnp.int32, (count, depth), 1).astype(f32)
-        chosen = jnp.concatenate(
-            [(spot == lut[:, r : r + 1]).astype(b16) for r in columns], axis=0
-        )
-
-        @pl.loop(0, width // tile_out)
-        def _(i):
-            cols = pl.ds(pl.multiple_of(i * tile_out, tile_out), tile_out)
-            results = store[:, :, cols].reshape(depth, tile_out)
-            picked = jnp.dot(chosen, results, preferred_element_type=f32)
-            found = lut[:, 4 + columns[0] : 5 + columns[0]] * picked[:count]
-            if c == "F":
-                found = found + lut[:, 7:8] * picked[count:]
-            if not opening:
-                found = acc[:, cols] + found
-            if closing:
-                expert_ref[:, cols] = found.astype(b16)
-            else:
-                acc[:, cols] = found
+            mixed_out.start()
+
+    def stage_pre():
+        spot = lax.broadcasted_iota(jnp.int32, (count, count), 1).astype(f32)
+        for r in range(4):
+            pick[r] = (spot == lut[:, r : r + 1]).astype(b16)
+
+    def stage_cmb():
+        for i in window:
+            near_back[i].wait_recv()
+        for p in range(blocks):
+            far_back(0, p).wait_recv()
+        for n in range(width // tile_out):
+            cols = slice(n * tile_out, (n + 1) * tile_out)
+            found = jnp.zeros((count, tile_out), f32)
+            for r, store in enumerate((oback, nback, fback, fback)):
+                depth = store.shape[0] * size
+                results = store[:, :, cols].reshape(depth, tile_out)
+                chosen = pick[r, :, :depth]
+                found += lut[:, 4 + r : 5 + r] * jnp.dot(
+                    chosen, results, preferred_element_type=f32
+                )
+            expert_ref[:, cols] = found.astype(b16)
+            expert_out[n].start()
 
     stages = {"A": stage_a, "B": stage_b, "C": stage_c, "D": stage_d, "E": stage_e}
     loaded = False
@@ -855,8 +872,10 @@
             stage_outp()
         elif name[:2] == "MX":
             stage_mx(int(name[2]))
-        elif name[:3] == "CMB":
-            stage_cmb(name[3])
+        elif name == "PRE":
+            stage_pre()
+        elif name == "CMB":
+            stage_cmb()
         elif name[0] == "Y":
             stage_y(int(name[1]))
         elif name[0] == "R":
@@ -866,7 +885,7 @@
         else:
             if name[0] == "C" and not loaded:
                 loaded = True
-                for n in (6, 7, 8):
+                for n in (11, 12, 13):
                     loads[n].wait()
             stages[name[0]](name[1:-1], int(name[-1]))
 
@@ -902,6 +921,9 @@
     for copy in m_core:
         copy.wait_send()
     m_x.wait_send()
+    mixed_out.wait()
+    for copy in expert_out:
+        copy.wait()
 
 
 def deliver_kernel(mixed_in, expert_in, mixed_out, expert_out, mixed_held, expert_held, sems):
@@ -969,7 +991,6 @@
     length, dim = projected_keys.shape
     kind = jnp.bfloat16
     cosine, sine = turn_tables(steps * length, dim)
-    vmem = pl.BlockSpec(memory_space=pltpu.VMEM)
     anywhere = pl.BlockSpec(memory_space=pltpu.HBM)
     units = 4 * wide
     mixed, expert = pl.pallas_call(
@@ -978,13 +999,17 @@
             jax.ShapeDtypeStruct((length // lanes, width), kind),
             jax.ShapeDtypeStruct((count, width), kind),
         ),
-        in_specs=[anywhere]
-        + [vmem] * 3
-        + [anywhere] * 7
-        + [vmem] * 2
-        + [anywhere] * 2,
-        out_specs=(vmem, vmem),
+        in_specs=[anywhere] * 15,
+        out_specs=(anywhere, anywhere),
         scratch_shapes=[
+            pltpu.VMEM((2, count), jnp.int32),
+            pltpu.VMEM((2, count), jnp.float32),
+            pltpu.VMEM((1, width), jnp.float32),
+            pltpu.VMEM((1, dim), jnp.float32),
+            pltpu.VMEM((1, dim), jnp.float32),
+            pltpu.VMEM((length // lanes, width), kind),
+            pltpu.VMEM((count, width), kind),
+            pltpu.VMEM((4, count, count), kind),
             pltpu.VMEM((width, hidden), kind),
             pltpu.VMEM((width, hidden), kind),
             pltpu.VMEM((hidden, width), kind),
@@ -1012,7 +1037,6 @@
             pltpu.VMEM((wide, size, width), kind),
             pltpu.VMEM((wide, size, width), kind),
             pltpu.VMEM((blocks, size, width), kind),
-            pltpu.VMEM((count, width), jnp.float32),
             pltpu.VMEM((count, count), jnp.float32),
             pltpu.VMEM((steps, 2, length, dim), kind),
             pltpu.VMEM(query_rows.shape, kind),
@@ -1020,7 +1044,8 @@
             pltpu.VMEM((2, length // lanes, width), kind),
             pltpu.VMEM((length // lanes, width), kind),
             pltpu.VMEM((length // lanes, width), kind),
-            pltpu.SemaphoreType.DMA((10,)),
+            pltpu.SemaphoreType.DMA((15,)),
+            pltpu.SemaphoreType.DMA((1 + width // math.gcd(width, 512),)),
         ]
         + [pltpu.SemaphoreType.DMA((2 * blocks,))] * 6
         + [pltpu.SemaphoreType.DMA((blocks + 2 * wide,))] * 2

time: 83.2 us -> 80.2 us (0.964)
  Pallas kernels: 82.4 us -> 79.4 us
    pallas_call x1, Pallas kernels: 80.5 us -> 77.5 us  [fused(): pl.pallas_call(functools.partial(fused_kernel, steps), out_shape=(jax.Sha...]
where the time goes in v3:
time: 80.2 us; the launch traced here: 80.1 us
  Pallas kernels  79.4 us (99%)
    pallas_call x1, Pallas kernels, fused(): pl.pallas_call(functools.partial(fused_kernel, steps), out_shape=(jax.Sha...  77.5 us
    pallas_call x1, Pallas kernels, fused(): pl.pallas_call(deliver_kernel, out_shape=(jax.ShapeDtypeStruct(mixed.shap...  1.95 us

profile of v3, /device:TPU:0, one launch (start us, length us, event | category | flops | bytes accessed | tf_op | source)
XLA Modules:
  0.0 80.1 jit_solution(15308505101021848367)
XLA Ops:
  0.6 77.5 %shard_map.158 = (bf16[48,2048]{1,0:T(8,128)(2,1)}, bf16[128,2048]{1,0:T(8,128)(2,1)}) custom-call(bf16[128,2048]{1,0:T(8,128)(2,1)} %tokens_hbm.1, s32[2,128]{1,0:T(2,128)} %bitcast.12, f32[2,128]{1,0:T(2,128)} %bitcast.13, f32[1,2048]{1,0:T(1,128)} %bitcast.11, bf16[2048,512]{1,0:T(8,128)(2,1)} %bitcast.8, bf16[2048,512]{1,0:T(8,128)(2,1)} %bitcast.9, ...), custom_call_target="tpu_custom_call" | custom-call | tf_op jit(solution)/shard_map/pallas_call | solution.py:996
  78.1 2.0 %shard_map.159 = (bf16[48,2048]{1,0:T(8,128)(2,1)}, bf16[128,2048]{1,0:T(8,128)(2,1)}) custom-call(bf16[48,2048]{1,0:T(8,128)(2,1)} %get-tuple-element.4.mixed_in, bf16[128,2048]{1,0:T(8,128)(2,1)} %get-tuple-element.5.expert_in), custom_call_target="tpu_custom_call" | custom-call | tf_op jit(solution)/shard_map/pallas_call | solution.py:1075

commit v4 on v3

--- a/solution.py
+++ b/solution.py
@@ -221,20 +221,21 @@
 
 
 ORDER = (
-    "SEND", "PRE", "BO2", "RF1", "CO2", "DO2", "AF10", "BO1", "RF0",
-    "AF11", "CO1", "AF00", "AF12", "BF11", "KV0", "AF01", "BF10", "Y1",
-    "Y0", "CF11", "CF10", "DF11", "KV1", "DF10", "BF12", "BF01", "BF00",
-    "Y2", "EO2", "CF12", "AF02", "EF11", "DF12", "KV2", "CF01", "BN0",
-    "CF00", "DF00", "DF01", "BF02", "DO1", "EF10", "EF12", "CF02", "BN1",
-    "CN0", "BN2", "ATT0", "GF10", "GF11", "EF00", "ATT1", "DF02", "GF12",
-    "BO0", "CN1", "DN0", "EF01", "GF00", "CN2", "DN1", "CO0", "EF02",
-    "ATT2", "EO1", "DN2", "ATT3", "DO0", "EN0", "EN1", "OUTP", "GF02",
-    "GF01", "EN2", "MX0", "EO0", "CMB", "MX1",
+    "SEND", "RF1", "BO2", "AF10", "CO2", "RF0", "AF11", "BF10", "AF00",
+    "BF11", "KV0", "PRE", "AF12", "CF11", "BO0", "AF01", "BF00", "CF10",
+    "DF11", "Y0", "KV1", "CF00", "Y1", "Y2", "BF01", "DF10", "BF12",
+    "CO0", "DF00", "AF02", "CF01", "BN0", "EF11", "CF12", "BN1", "CN0",
+    "KV2", "EF00", "DF01", "DF12", "CN1", "EF10", "GF11", "BF02", "BN2",
+    "DO2", "EF01", "BO1", "GF00", "DN0", "DN1", "CF02", "GF10", "DF02",
+    "EF12", "CN2", "ATT0", "GF01", "DN2", "EN1", "CO1", "ATT1", "ATT2",
+    "EF02", "ATT3", "DO0", "OUTP", "DO1", "EN2", "EN0", "GF12", "EO2",
+    "GF02", "EO0", "MX0", "EO1", "CMBP", "CMB", "MX1",
 )
 SENDS = (
-    ("F", 0), ("F", 1), ("N", 0), ("F", 2), ("N", 1),
-    ("X", 3), ("N", 2), ("F", 3), ("X", 2), ("X", 1), ("X", 0),
+    ("X", 2), ("X", 3), ("N", 2), ("F", 0), ("F", 1),
+    ("F", 2), ("N", 1), ("F", 3), ("X", 1), ("N", 0), ("X", 0),
 )
+SHARED_PIECE = 1
 VMEM_LIMIT = 58 * 1024 * 1024
 
 
@@ -278,6 +279,11 @@
     outf,
     scl,
     sc,
+    own_scl,
+    x_scl,
+    near_two,
+    near_got,
+    own_sum,
     orows,
     nrows,
     frows,
@@ -292,6 +298,7 @@
     oback,
     nback,
     fback,
+    acc,
     lut,
     kv,
     heads_ref,
@@ -323,6 +330,8 @@
     fb_r,
     sc_s,
     sc_r,
+    ns_s,
+    ns_r,
     ks,
     kr,
     ms,
@@ -353,7 +362,6 @@
             [
                 (ids_hbm, ids_ref),
                 (score_hbm, score_ref),
-                (tokens_hbm, tok_ref),
                 (ngain_hbm, ngain_ref),
                 (kgain_hbm, kgain_ref),
                 (key_hbm, keyraw_ref),
@@ -369,14 +377,27 @@
             ]
         )
     ]
-    for load in loads:
+    spots = [pl.ds(n * size, size) for n in range(blocks)]
+    pieces = [
+        pltpu.make_async_copy(tokens_hbm.at[spot], tok_ref.at[spot], hsem.at[len(loads) + n])
+        for n, spot in enumerate(spots)
+    ]
+    for load in loads[:3] + pieces + loads[3:]:
         load.start()
 
     barrier = pltpu.get_barrier_semaphore()
-    friends = [{"ep": peers[k], "tp": lane} for k in range(1, steps)]
-    friends += [{"ep": me, "tp": core}, {"ep": me, "tp": across}]
+    friends = [{"ep": me, "tp": core}, {"ep": me, "tp": across}]
+    friends += [{"ep": peers[k], "tp": lane} for k in (1, 2)]
+
+    def greet(friend):
+        pl.semaphore_signal(barrier, inc=1, device_id=friend, device_id_type=MESH)
+
+    @pl.when(inner == 1)
+    def _():
+        greet({"ep": peers[3], "tp": lane})
+
     for friend in friends:
-        pl.semaphore_signal(barrier, inc=1, device_id=friend, device_id_type=MESH)
+        greet(friend)
 
     def remote(src, dst, send, recv, ep_to, tp_to):
         return pltpu.make_async_remote_copy(
@@ -398,6 +419,16 @@
     window = range(wide)
     number = {(c, i): n * wide + i for n, c in enumerate(kinds) for i in window}
 
+    def by_role(i, special, usual):
+        if i == SHARED_PIECE - 1:
+            when_inner(special)
+            when_outer(usual)
+        elif i == SHARED_PIECE:
+            when_outer(special)
+            when_inner(usual)
+        else:
+            usual()
+
     def rows_of(c, i):
         if c == "O":
             return orows.at[i + inner]
@@ -406,14 +437,14 @@
         return frows.at[int(c[1]), i + inner]
 
     def x_own(p):
-        return remote(orows.at[p, 0], orows.at[p, 1], xs.at[p], xr.at[p], me, across)
+        return remote(orows.at[p, 0], orows.at[p, 1], xs.at[0], xr.at[p], me, across)
 
     near = [
         [
             remote(
                 orows.at[i + outer, n],
                 nrows.at[i, n],
-                near_s.at[n * wide + i],
+                near_s.at[0],
                 near_r.at[n * wide + i],
                 peers[1],
                 lane,
@@ -426,7 +457,7 @@
         remote(
             outf.at[p],
             frows.at[outer, p, 0],
-            far_s.at[p],
+            far_s.at[0],
             far_r.at[outer * blocks + p],
             gate_at,
             lane,
@@ -436,7 +467,7 @@
     far_in = [
         [
             remote(
-                outf.at[p], frows.at[j, p, 0], far_s.at[p], far_r.at[j * blocks + p], gate_at, lane
+                outf.at[p], frows.at[j, p, 0], far_s.at[0], far_r.at[j * blocks + p], gate_at, lane
             )
             for p in range(blocks)
         ]
@@ -447,7 +478,7 @@
             remote(
                 frows.at[j, p, 0],
                 frows.at[j, p, 0],
-                rel_s.at[j * wide + p],
+                rel_s.at[0],
                 rel_r.at[j * wide + p],
                 peers[1],
                 lane,
@@ -463,24 +494,26 @@
         held = rows_of(c, i)
         if c[0] == "F":
             at = blocks + u - 2 * wide
-            x_far[c, i] = remote(held.at[0], held.at[1], xs.at[at], xr.at[at], me, across)
+            x_far[c, i] = remote(held.at[0], held.at[1], xs.at[0], xr.at[at], me, across)
         c_in[c, i] = remote(
-            held.at[pl.ds(0, 2)], held.at[pl.ds(2, 2)], cs.at[u], cr.at[u], me, core
+            held.at[pl.ds(0, 2)], held.at[pl.ds(2, 2)], cs.at[0], cr.at[u], me, core
         )
         c_out[c, i] = remote(
-            part.at[u, pl.ds(2, 2)], from_core.at[u], ps.at[u], pr.at[u], me, core
-        )
-        x_out[c, i] = remote(to_x.at[u], from_x.at[u], qs.at[u], qr.at[u], me, across)
+            part.at[u, pl.ds(2, 2)], from_core.at[u], ps.at[0], pr.at[u], me, core
+        )
+        x_out[c, i] = remote(to_x.at[u], from_x.at[u], qs.at[0], qr.at[u], me, across)
     near_back = [
-        remote(total.at[wide + i], nback.at[i], nb_s.at[i], nb_r.at[i], peers[1], lane)
+        remote(total.at[wide + i], nback.at[i], nb_s.at[0], nb_r.at[i], peers[1], lane)
         for i in window
     ]
+    near_sum = remote(near_two, near_got, ns_s.at[0], ns_r.at[0], peers[1], lane)
+    own_scale = remote(own_scl, x_scl, ns_s.at[1], ns_r.at[1], me, across)
     far_over = [
         [
             remote(
                 total.at[(2 + j) * wide + i],
                 fres.at[j, i],
-                fo_s.at[j * wide + i],
+                fo_s.at[0],
                 fo_r.at[j * wide + i],
                 peers[1],
                 lane,
@@ -498,7 +531,7 @@
         else:
             source = comb.at[j, p - 1]
         return remote(
-            source, fback.at[p], fb_s.at[j * blocks + p], fb_r.at[p], sources[j], lane
+            source, fback.at[p], fb_s.at[0], fb_r.at[p], sources[j], lane
         )
 
     kv_near = remote(kv.at[0], kv.at[1], ks.at[0], kr.at[0], peers[1], lane)
@@ -506,9 +539,9 @@
     kv_far = remote(kv.at[pl.ds(2, 2)], kv.at[pl.ds(2, 2)], ks.at[2], kr.at[2], peers[1], lane)
     m_core = [
         remote(pm.at[core], fc.at[0], ms.at[0], mr.at[0], me, core),
-        remote(pm.at[flip(core, 2)], fc.at[1], ms.at[1], mr.at[1], me, core),
+        remote(pm.at[flip(core, 2)], fc.at[1], ms.at[0], mr.at[1], me, core),
     ]
-    m_x = remote(to_xm, from_xm, ms.at[2], mr.at[2], me, across)
+    m_x = remote(to_xm, from_xm, ms.at[1], mr.at[2], me, across)
     mixed_out = pltpu.make_async_copy(mixed_ref, mixed_hbm, osem.at[0])
     expert_out = [
         pltpu.make_async_copy(
@@ -575,7 +608,7 @@
         mid_pos = jnp.where(mid_only + both > 0.5, mid_pos, -1.0)
         return end_pos, mid_pos, jnp.where((both > 0.5) & shared, 1.0, 0.0)
 
-    own_end, own_mid, _ = positions(0)
+    own_end, own_mid, own_shared = positions(0)
     far_end, far_mid, far_shared = positions(1)
     slot = lax.broadcasted_iota(jnp.int32, (count, count), 0).astype(f32)
 
@@ -585,26 +618,33 @@
         return picked.astype(b16).reshape(blocks, size, width)
 
     loads[2].wait()
-    loads[3].wait()
-    for n in range(blocks):
-        spot = pl.ds(n * size, size)
+    for n, spot in enumerate(spots):
+        pieces[n].wait()
         values = tok_ref[spot, :].astype(f32)
         norm_ref[spot, :] = (
             values
             * lax.rsqrt(jnp.mean(values * values, axis=-1, keepdims=True) + EPS)
             * ngain_ref[...]
         ).astype(b16)
+    orows[:, 0] = dispatch(own_end, own_mid)
+
+    @when_inner
+    def _():
+        pl.semaphore_wait(barrier, len(friends) + 1)
+
+    @when_outer
+    def _():
+        pl.semaphore_wait(barrier, len(friends))
+
+    for kind, p in SENDS:
+        if kind == "X":
+            x_own(p).start()
     outf[...] = dispatch(far_end, far_mid)
-    pl.semaphore_wait(barrier, len(friends))
-    far[0].start()
-    orows[:, 0] = dispatch(own_end, own_mid)
 
     def stage_send():
         for kind, p in SENDS:
-            if kind == "F" and p > 0:
+            if kind == "F":
                 far[p].start()
-            elif kind == "X":
-                x_own(p).start()
             elif kind == "N":
                 near[0][p].start()
         end_share, mid_share = named[1][0][1], named[1][1][1]
@@ -627,14 +667,42 @@
         scl[...] = jnp.where(lanes_of < scl.shape[1] // 2, end_scale, mid_scale)
         scale_out.start()
         is_inner = (jnp.zeros((1, count), jnp.int32) + inner) == 1
-        own_mid_at = jnp.where(own_mid < 0.0, -1.0, own_mid - tail)
+        own_at = jnp.where(is_inner, own_mid, own_end)
+        near_at = jnp.where(is_inner, own_end, own_mid)
+        own_share = jnp.where(is_inner, named[0][1][1], named[0][0][1])
+        near_share = jnp.where(is_inner, named[0][0][1], named[0][1][1])
+        rows_one = slice(size * SHARED_PIECE, size * (SHARED_PIECE + 1))
+        own_factor = jnp.sum(
+            jnp.where(
+                slot[rows_one] == own_at, jnp.where(own_shared > 0.5, own_share, 1.0), 0.0
+            ),
+            axis=1,
+            keepdims=True,
+        )
+        near_factor = jnp.sum(
+            jnp.where(
+                slot[rows_one] == near_at, jnp.where(own_shared > 0.5, near_share, 1.0), 0.0
+            ),
+            axis=1,
+            keepdims=True,
+        )
+        lanes_one = lax.broadcasted_iota(jnp.int32, own_scl.shape, 1)
+        own_scl[...] = jnp.where(lanes_one < own_scl.shape[1] // 2, own_factor, near_factor)
+        own_scale.start()
+        nback[SHARED_PIECE - outer] = jnp.zeros((size, width), b16)
+        moved = (near_at >= size * SHARED_PIECE) & (near_at < size * (SHARED_PIECE + 1))
+        own_first = jnp.where(is_inner, tail, 0.0)
+        own_held = jnp.where(moved, near_at, own_at)
+        near_held = jnp.where(moved, -1.0, near_at)
         table = (
-            jnp.where(is_inner, own_mid_at, own_end),
-            jnp.where(is_inner, own_end, own_mid_at),
+            jnp.where(own_held < 0.0, -1.0, own_held - own_first),
+            jnp.where(near_held < 0.0, -1.0, near_held - (tail - own_first)),
             far_end,
             jnp.where(far_shared > 0.5, -1.0, far_mid),
-            jnp.where(is_inner, named[0][1][1], named[0][0][1]),
-            jnp.where(is_inner, named[0][0][1], named[0][1][1]),
+            jnp.where(
+                moved, jnp.where(own_shared > 0.5, 1.0, near_share), own_share
+            ),
+            near_share,
             jnp.where(far_shared > 0.5, 1.0, end_share),
             mid_share,
         )
@@ -734,22 +802,70 @@
     def stage_d(c, i):
         c_out[c, i].wait_recv()
         u = number[c, i]
-        to_x[u] = (part[u, 1].astype(f32) + from_core[u, 1].astype(f32)).astype(b16)
-        x_out[c, i].start()
+
+        def usual():
+            to_x[u] = (part[u, 1].astype(f32) + from_core[u, 1].astype(f32)).astype(b16)
+            x_out[c, i].start()
+
+        def near_special():
+            for n in range(2):
+                near_two[n] = (
+                    part[u, n].astype(f32) + from_core[u, n].astype(f32)
+                ).astype(b16)
+            near_sum.start()
+
+        def own_special():
+            near_sum.wait_recv()
+            own_scale.wait_recv()
+            half = own_scl.shape[1] // 2
+            for n, factors in ((1, x_scl), (0, own_scl)):
+                both = factors[:, 0:1] * (
+                    part[u, n].astype(f32) + from_core[u, n].astype(f32)
+                ) + factors[:, half : half + 1] * near_got[n].astype(f32)
+                if n:
+                    to_x[u] = both.astype(b16)
+                    x_out[c, i].start()
+                else:
+                    own_sum[...] = both
+
+        if c == "N":
+            by_role(i, near_special, usual)
+        elif c == "O":
+            by_role(i, own_special, usual)
+        else:
+            usual()
 
     def stage_e(c, i):
-        x_out[c, i].wait_recv()
         u = number[c, i]
-        summed = (
-            part[u, 0].astype(f32) + from_core[u, 0].astype(f32) + from_x[u].astype(f32)
-        ).astype(b16)
+
+        def reduced():
+            x_out[c, i].wait_recv()
+            return (
+                part[u, 0].astype(f32)
+                + from_core[u, 0].astype(f32)
+                + from_x[u].astype(f32)
+            ).astype(b16)
+
         if c == "O":
-            oback[i] = summed
+
+            def own_special():
+                x_out[c, i].wait_recv()
+                oback[i] = (own_sum[...] + from_x[u].astype(f32)).astype(b16)
+
+            def own_usual():
+                oback[i] = reduced()
+
+            by_role(i, own_special, own_usual)
             return
-        total[u] = summed
         if c == "N":
-            near_back[i].start()
+
+            def near_usual():
+                total[u] = reduced()
+                near_back[i].start()
+
+            by_role(i, lambda: None, near_usual)
             return
+        total[u] = reduced()
         j = int(c[1])
         when_outer(far_over[j][i].start)
         if i == wide - 1:
@@ -775,7 +891,7 @@
 
     def stage_kv(step):
         if step == 0:
-            for n in range(4, 9):
+            for n in range(3, 8):
                 loads[n].wait()
             kv[0, 0] = turned(keyraw_ref[...], kgain_ref)
             kv_near.start()
@@ -791,8 +907,8 @@
 
     def stage_att(head):
         if head == 0:
+            loads[8].wait()
             loads[9].wait()
-            loads[10].wait()
             when_outer(kv_far.wait_recv)
         cols = slice(head * dim, (head + 1) * dim)
         held = steps * length
@@ -812,7 +928,7 @@
         heads_ref[:, cols] = (summed / amount).astype(b16)
 
     def stage_outp():
-        loads[14].wait()
+        loads[13].wait()
 
         @pl.loop(0, width // tile_out)
         def _(i):
@@ -841,23 +957,38 @@
         for r in range(4):
             pick[r] = (spot == lut[:, r : r + 1]).astype(b16)
 
-    def stage_cmb():
+    def gathered(cols, stores):
+        found = 0.0
+        for r, store in stores:
+            depth = store.shape[0] * size
+            results = store[:, :, cols].reshape(depth, tile_out)
+            found += lut[:, 4 + r : 5 + r] * jnp.dot(
+                pick[r, :, :depth], results, preferred_element_type=f32
+            )
+        return found
+
+    def stage_cmb(last):
+        if last:
+            for n in range(width // tile_out):
+                cols = slice(n * tile_out, (n + 1) * tile_out)
+                found = acc[:, cols] + gathered(cols, ((0, oback),))
+                expert_ref[:, cols] = found.astype(b16)
+                expert_out[n].start()
+            return
         for i in window:
-            near_back[i].wait_recv()
+            if i == SHARED_PIECE - 1:
+                when_inner(near_back[i].wait_recv)
+            elif i == SHARED_PIECE:
+                when_outer(near_back[i].wait_recv)
+            else:
+                near_back[i].wait_recv()
         for p in range(blocks):
             far_back(0, p).wait_recv()
-        for n in range(width // tile_out):
-            cols = slice(n * tile_out, (n + 1) * tile_out)
-            found = jnp.zeros((count, tile_out), f32)
-            for r, store in enumerate((oback, nback, fback, fback)):
-                depth = store.shape[0] * size
-                results = store[:, :, cols].reshape(depth, tile_out)
-                chosen = pick[r, :, :depth]
-                found += lut[:, 4 + r : 5 + r] * jnp.dot(
-                    chosen, results, preferred_element_type=f32
-                )
-            expert_ref[:, cols] = found.astype(b16)
-            expert_out[n].start()
+
+        @pl.loop(0, width // tile_out)
+        def _(n):
+            cols = pl.ds(pl.multiple_of(n * tile_out, tile_out), tile_out)
+            acc[:, cols] = gathered(cols, ((1, nback), (2, fback), (3, fback)))
 
     stages = {"A": stage_a, "B": stage_b, "C": stage_c, "D": stage_d, "E": stage_e}
     loaded = False
@@ -874,8 +1005,8 @@
             stage_mx(int(name[2]))
         elif name == "PRE":
             stage_pre()
-        elif name == "CMB":
-            stage_cmb()
+        elif name[:3] == "CMB":
+            stage_cmb(name == "CMB")
         elif name[0] == "Y":
             stage_y(int(name[1]))
         elif name[0] == "R":
@@ -885,20 +1016,25 @@
         else:
             if name[0] == "C" and not loaded:
                 loaded = True
-                for n in (11, 12, 13):
+                for n in (10, 11, 12):
                     loads[n].wait()
             stages[name[0]](name[1:-1], int(name[-1]))
 
-    for p in range(blocks):
-        x_own(p).wait_send()
-        far[p].wait_send()
-    for table in (x_far, c_in, c_out, x_out):
-        for copy in table.values():
-            copy.wait_send()
-    for i in window:
-        near[0][i].wait_send()
-        near[1][i].wait_send()
-        near_back[i].wait_send()
+    def all_sent(sem, like):
+        pltpu.make_async_copy(like, like, sem).wait()
+
+    def some(n):
+        return total.at[pl.ds(0, n)]
+
+    all_sent(xs.at[0], some(blocks + 2 * wide))
+    all_sent(cs.at[0], from_core)
+    all_sent(ps.at[0], from_core)
+    all_sent(qs.at[0], some(4 * wide - 1))
+    all_sent(near_s.at[0], some(2 * wide))
+    all_sent(far_s.at[0], some(blocks))
+    all_sent(nb_s.at[0], some(wide - 1))
+    near_sum.wait_send()
+    own_scale.wait_send()
     scale_out.wait_send()
     kv_near.wait_send()
 
@@ -906,20 +1042,14 @@
     def _():
         kv_mid.wait_send()
         kv_far.wait_send()
-        for j in range(2):
-            for i in window:
-                relay[j][i].wait_send()
-            for p in range(blocks):
-                far_back(j, p).wait_send()
+        all_sent(rel_s.at[0], some(2 * wide))
+        all_sent(fb_s.at[0], some(2 * blocks))
 
     @when_outer
     def _():
-        for j in range(2):
-            for i in window:
-                far_over[j][i].wait_send()
-
-    for copy in m_core:
-        copy.wait_send()
+        all_sent(fo_s.at[0], some(2 * wide))
+
+    all_sent(ms.at[0], fc)
     m_x.wait_send()
     mixed_out.wait()
     for copy in expert_out:
@@ -1023,6 +1153,11 @@
             pltpu.VMEM((blocks, size, width), kind),
             pltpu.VMEM((size * (wide - 1), 128), jnp.float32),
             pltpu.VMEM((2, size * (wide - 1), 128), jnp.float32),
+            pltpu.VMEM((size, 128), jnp.float32),
+            pltpu.VMEM((size, 128), jnp.float32),
+            pltpu.VMEM((2, size, width), kind),
+            pltpu.VMEM((2, size, width), kind),
+            pltpu.VMEM((size, width), jnp.float32),
             pltpu.VMEM((blocks, 4, size, width), kind),
             pltpu.VMEM((wide, 4, size, width), kind),
             pltpu.VMEM((2, blocks, 4, size, width), kind),
@@ -1037,6 +1172,7 @@
             pltpu.VMEM((wide, size, width), kind),
             pltpu.VMEM((wide, size, width), kind),
             pltpu.VMEM((blocks, size, width), kind),
+            pltpu.VMEM((count, width), jnp.float32),
             pltpu.VMEM((count, count), jnp.float32),
             pltpu.VMEM((steps, 2, length, dim), kind),
             pltpu.VMEM(query_rows.shape, kind),
@@ -1044,14 +1180,17 @@
             pltpu.VMEM((2, length // lanes, width), kind),
             pltpu.VMEM((length // lanes, width), kind),
             pltpu.VMEM((length // lanes, width), kind),
-            pltpu.SemaphoreType.DMA((15,)),
+            pltpu.SemaphoreType.DMA((14 + blocks,)),
             pltpu.SemaphoreType.DMA((1 + width // math.gcd(width, 512),)),
         ]
-        + [pltpu.SemaphoreType.DMA((2 * blocks,))] * 6
-        + [pltpu.SemaphoreType.DMA((blocks + 2 * wide,))] * 2
-        + [pltpu.SemaphoreType.DMA((units,))] * 6
-        + [pltpu.SemaphoreType.DMA((2 * blocks,))] * 6
-        + [pltpu.SemaphoreType.DMA((3,))] * 6,
+        + [
+            pltpu.SemaphoreType.DMA((n,))
+            for n in (1, 2 * wide, 1, 2 * blocks, 1, 2 * wide)
+            + (1, blocks + 2 * wide)
+            + (1, units) * 3
+            + (1, wide, 1, 2 * wide, 1, blocks)
+            + (1, 2, 2, 2, 3, 3, 2, 3)
+        ],
         compiler_params=pltpu.CompilerParams(
             collective_id=0, has_side_effects=True, vmem_limit_bytes=VMEM_LIMIT
         ),

time: 80.2 us -> 77.9 us (0.971)
  Pallas kernels: 79.4 us -> 77.1 us
    pallas_call x1, Pallas kernels: 77.5 us -> 75.2 us  [fused(): pl.pallas_call(functools.partial(fused_kernel, steps), out_shape=(jax.Sha...]
where the time goes in v4:
time: 77.9 us; the launch traced here: 77.8 us
  Pallas kernels  77.1 us (99%)
    pallas_call x1, Pallas kernels, fused(): pl.pallas_call(functools.partial(fused_kernel, steps), out_shape=(jax.Sha...  75.2 us
    pallas_call x1, Pallas kernels, fused(): pl.pallas_call(deliver_kernel, out_shape=(jax.ShapeDtypeStruct(mixed.shap...  1.95 us

profile of v4, /device:TPU:0, one launch (start us, length us, event | category | flops | bytes accessed | tf_op | source)
XLA Modules:
  0.0 77.8 jit_solution(14680969267736516368)
XLA Ops:
  0.6 75.2 %shard_map.158 = (bf16[48,2048]{1,0:T(8,128)(2,1)}, bf16[128,2048]{1,0:T(8,128)(2,1)}) custom-call(bf16[128,2048]{1,0:T(8,128)(2,1)} %tokens_hbm.1, s32[2,128]{1,0:T(2,128)} %bitcast.12, f32[2,128]{1,0:T(2,128)} %bitcast.13, f32[1,2048]{1,0:T(1,128)} %bitcast.11, bf16[2048,512]{1,0:T(8,128)(2,1)} %bitcast.8, bf16[2048,512]{1,0:T(8,128)(2,1)} %bitcast.9, ...), custom_call_target="tpu_custom_call" | custom-call | tf_op jit(solution)/shard_map/pallas_call | solution.py:1126
  75.8 2.0 %shard_map.159 = (bf16[48,2048]{1,0:T(8,128)(2,1)}, bf16[128,2048]{1,0:T(8,128)(2,1)}) custom-call(bf16[48,2048]{1,0:T(8,128)(2,1)} %get-tuple-element.4.mixed_in, bf16[128,2048]{1,0:T(8,128)(2,1)} %get-tuple-element.5.expert_in), custom_call_target="tpu_custom_call" | custom-call | tf_op jit(solution)/shard_map/pallas_call | solution.py:1214

commit v5 on v4

--- a/solution.py
+++ b/solution.py
@@ -229,7 +229,7 @@
     "DO2", "EF01", "BO1", "GF00", "DN0", "DN1", "CF02", "GF10", "DF02",
     "EF12", "CN2", "ATT0", "GF01", "DN2", "EN1", "CO1", "ATT1", "ATT2",
     "EF02", "ATT3", "DO0", "OUTP", "DO1", "EN2", "EN0", "GF12", "EO2",
-    "GF02", "EO0", "MX0", "EO1", "CMBP", "CMB", "MX1",
+    "GF02", "EO0", "MX0", "EO1", "CMB", "MX1",
 )
 SENDS = (
     ("X", 2), ("X", 3), ("N", 2), ("F", 0), ("F", 1),
@@ -298,7 +298,6 @@
     oback,
     nback,
     fback,
-    acc,
     lut,
     kv,
     heads_ref,
@@ -351,7 +350,7 @@
     length = query_ref.shape[0]
     dim = keyraw_ref.shape[1]
     count = tok_ref.shape[0]
-    tile = math.gcd(hidden, 256)
+    tile = math.gcd(hidden, 512)
     tile_out = math.gcd(width, 512)
     f32, b16 = jnp.float32, jnp.bfloat16
 
@@ -479,7 +478,7 @@
                 frows.at[j, p, 0],
                 frows.at[j, p, 0],
                 rel_s.at[0],
-                rel_r.at[j * wide + p],
+                far_r.at[j * blocks + p],
                 peers[1],
                 lane,
             )
@@ -967,14 +966,7 @@
             )
         return found
 
-    def stage_cmb(last):
-        if last:
-            for n in range(width // tile_out):
-                cols = slice(n * tile_out, (n + 1) * tile_out)
-                found = acc[:, cols] + gathered(cols, ((0, oback),))
-                expert_ref[:, cols] = found.astype(b16)
-                expert_out[n].start()
-            return
+    def stage_cmb():
         for i in window:
             if i == SHARED_PIECE - 1:
                 when_inner(near_back[i].wait_recv)
@@ -984,11 +976,11 @@
                 near_back[i].wait_recv()
         for p in range(blocks):
             far_back(0, p).wait_recv()
-
-        @pl.loop(0, width // tile_out)
-        def _(n):
-            cols = pl.ds(pl.multiple_of(n * tile_out, tile_out), tile_out)
-            acc[:, cols] = gathered(cols, ((1, nback), (2, fback), (3, fback)))
+        for n in range(width // tile_out):
+            cols = slice(n * tile_out, (n + 1) * tile_out)
+            found = gathered(cols, ((0, oback), (1, nback), (2, fback), (3, fback)))
+            expert_ref[:, cols] = found.astype(b16)
+            expert_out[n].start()
 
     stages = {"A": stage_a, "B": stage_b, "C": stage_c, "D": stage_d, "E": stage_e}
     loaded = False
@@ -1005,8 +997,8 @@
             stage_mx(int(name[2]))
         elif name == "PRE":
             stage_pre()
-        elif name[:3] == "CMB":
-            stage_cmb(name == "CMB")
+        elif name == "CMB":
+            stage_cmb()
         elif name[0] == "Y":
             stage_y(int(name[1]))
         elif name[0] == "R":
@@ -1059,7 +1051,7 @@
 def deliver_kernel(mixed_in, expert_in, mixed_out, expert_out, mixed_held, expert_held, sems):
     pairs = []
     for source, held, target, pieces in (
-        (expert_in, expert_held, expert_out, 4),
+        (expert_in, expert_held, expert_out, 1),
         (mixed_in, mixed_held, mixed_out, 1),
     ):
         size = source.shape[0] // pieces
@@ -1172,7 +1164,6 @@
             pltpu.VMEM((wide, size, width), kind),
             pltpu.VMEM((wide, size, width), kind),
             pltpu.VMEM((blocks, size, width), kind),
-            pltpu.VMEM((count, width), jnp.float32),
             pltpu.VMEM((count, count), jnp.float32),
             pltpu.VMEM((steps, 2, length, dim), kind),
             pltpu.VMEM(query_rows.shape, kind),
@@ -1185,7 +1176,7 @@
         ]
         + [
             pltpu.SemaphoreType.DMA((n,))
-            for n in (1, 2 * wide, 1, 2 * blocks, 1, 2 * wide)
+            for n in (1, 2 * wide, 1, 2 * blocks, 1, 1)
             + (1, blocks + 2 * wide)
             + (1, units) * 3
             + (1, wide, 1, 2 * wide, 1, blocks)
@@ -1222,7 +1213,7 @@
         scratch_shapes=[
             pltpu.VMEM(mixed.shape, kind),
             pltpu.VMEM(expert.shape, kind),
-            pltpu.SemaphoreType.DMA((2, 5)),
+            pltpu.SemaphoreType.DMA((2, 2)),
         ],
     )(mixed, expert)
 

time: 77.9 us -> 77.7 us (level)
  no operation moved by 1% of the time
where the time goes in v5:
time: 77.7 us; the launch traced here: 77.5 us
  Pallas kernels  76.7 us (99%)
  between operations  0.8 us (1%)
    pallas_call x1, Pallas kernels, fused(): pl.pallas_call(functools.partial(fused_kernel, steps), out_shape=(jax.Sha...  74.8 us
    pallas_call x1, Pallas kernels, fused(): pl.pallas_call(deliver_kernel, out_shape=(jax.ShapeDtypeStruct(mixed.shap...  1.93 us

profile of v5, /device:TPU:0, one launch (start us, length us, event | category | flops | bytes accessed | tf_op | source)
XLA Modules:
  0.0 77.5 jit_solution(245532590757268710)
XLA Ops:
  0.6 74.8 %shard_map.158 = (bf16[48,2048]{1,0:T(8,128)(2,1)}, bf16[128,2048]{1,0:T(8,128)(2,1)}) custom-call(bf16[128,2048]{1,0:T(8,128)(2,1)} %tokens_hbm.1, s32[2,128]{1,0:T(2,128)} %bitcast.12, f32[2,128]{1,0:T(2,128)} %bitcast.13, f32[1,2048]{1,0:T(1,128)} %bitcast.11, bf16[2048,512]{1,0:T(8,128)(2,1)} %bitcast.8, bf16[2048,512]{1,0:T(8,128)(2,1)} %bitcast.9, ...), custom_call_target="tpu_custom_call" | custom-call | tf_op jit(solution)/shard_map/pallas_call | solution.py:1118
  75.4 1.9 %shard_map.159 = (bf16[48,2048]{1,0:T(8,128)(2,1)}, bf16[128,2048]{1,0:T(8,128)(2,1)}) custom-call(bf16[48,2048]{1,0:T(8,128)(2,1)} %get-tuple-element.4.mixed_in, bf16[128,2048]{1,0:T(8,128)(2,1)} %get-tuple-element.5.expert_in), custom_call_target="tpu_custom_call" | custom-call | tf_op jit(solution)/shard_map/pallas_call | solution.py:1205
